TPU v7x, 128 devices: a whole 4x4x4 slice. The times are simulated.
128 devices in a mesh: sp: 16 (over z, x), tp: 8 (over y, core).
Axes of the slice: x: 4, y: 4, z: 4, core: 2. Of those that a mesh axis runs over, the one named last changes fastest.
Arguments:
- tokens: bfloat16 [12288, 4096], P('sp', 'tp'), may hold values from -12 to 12
- query_weight: bfloat16 [4096, 2048], P(None, 'tp'), may hold values from -0.09375 to 0.09375
- key_weight: bfloat16 [4096, 2048], P(None, 'tp'), may hold values from -0.09375 to 0.09375
- value_weight: bfloat16 [4096, 2048], P(None, 'tp'), may hold values from -0.09375 to 0.09375
- position_bias: float32 [16, 320], P('tp'), may hold values from -104 to 154
- out_grad: bfloat16 [12288, 2048], P('sp', 'tp'), may hold values from -6 to 6
Outputs:
- input_grad: bfloat16 [12288, 4096], P('sp', 'tp')
- query_weight_grad: float32 [4096, 2048], P('sp', 'tp')
- key_weight_grad: float32 [4096, 2048], P('sp', 'tp')
- value_weight_grad: float32 [4096, 2048], P('sp', 'tp')
- bias_grad: float32 [16, 320], P('tp')
All inputs are finite; a program needn't handle non-finite values.
Results may differ from a plain program's by a relative error of at most 0.014.
Values may be sent and summed in bfloat16 or wider, within the bound.
A program may use at most 128 MiB of HBM per device.

v0:
```python
import functools

import jax
import jax.numpy as jnp
from jax import lax
from jax.experimental import pallas as pl
from jax.experimental.pallas import tpu as pltpu
from jax.sharding import PartitionSpec as P

MESH = pl.DeviceIdType.MESH
BF16, F32 = jnp.bfloat16, jnp.float32
SEGMENT, REACH, CLIP, HEAD = 64, 256, 256, 128
TILE = 128
SPAN = REACH + TILE
LENGTH, WIDTH, FEATURES = 768, 4096, 512
CHUNKS = LENGTH // TILE
HEADS = 2
COLS = HEADS * HEAD
FACTOR = HEAD ** (-0.5)
RING = 4
TABLE = 320
ROUND = 512


def dot(left, right, left_dim=1, right_dim=0):
    return lax.dot_general(left, right, (((left_dim,), (right_dim,)), ((), ())), preferred_element_type=F32)


class Ring:
    def __init__(self, me, up, down, block, via, direct, joined, sems):
        self.near = (lax.rem(me + 1, RING), lax.rem(me + RING - 1, RING))
        self.far = lax.rem(me + 2, RING)
        self.me, self.devices, self.block = me, (up, down), block
        self.landing, self.sems = (via, direct, joined), sems

    def copy(self, kind, d):
        source = (self.block(self.far, d), self.block(self.near[d], 1 - d), self.block(self.near[d], d))[kind]
        send, recv = self.sems
        return pltpu.make_async_remote_copy(
            src_ref=source,
            dst_ref=self.landing[kind](d),
            send_sem=send(kind, d),
            recv_sem=recv(kind, d),
            device_id=self.devices[d],
            device_id_type=MESH,
        )

    def start_far(self):
        for d in range(2):
            self.copy(0, d).start()

    def start_near(self, d):
        self.copy(1, d).start()

    def join(self):
        for d in range(2):
            self.copy(0, d).wait_recv()
            ref = self.block(self.near[d], d)
            ref[...] = (ref[...].astype(F32) + self.landing[0](d)[...].astype(F32)).astype(BF16)
            self.copy(2, d).start()

    def half(self, d):
        self.copy(2, d).wait_recv()
        self.copy(1, 1 - d).wait_recv()
        total = self.block(self.me, d)[...].astype(F32) + self.landing[2](d)[...].astype(F32)
        return total + self.landing[1](1 - d)[...].astype(F32)

    def wait_sends(self):
        for kind in range(3):
            for d in range(2):
                self.copy(kind, d).wait_send()


def kernel(
    tokens, wq, wk, wv, table, out_grad,
    input_out, wq_out, wk_out, wv_out, bias_out,
    whole, weight, query, kv, upstream, dkv, grads, grads_t, back_send, back_recv,
    part_a, part_b, far_ab, near_ab, join_ab, second_ab, far2_ab, near2_ab, join2_ab,
    term_own, term_send, term_recv, far_y, near_y, join_y,
    input_stage, weight_stage, bias, dsum, bias_x, bias_z,
    load_sem, gather_send, gather_recv, hop_send, hop_recv, core_send, core_recv,
    halo_send, halo_recv, back_sems, term_ss, term_rs, ring_ss, ring_rs, y_ss, y_rs, bx_s, bx_r, bz_s, bz_r, store_sem,
):
    sp, tp = lax.axis_index("sp"), lax.axis_index("tp")
    z, x = sp // RING, lax.rem(sp, RING)
    y, core = tp // 2, lax.rem(tp, 2)

    def at(value, by):
        return lax.rem(value + by, RING)

    def at_x(by):
        return (z * RING + at(x, by), tp)

    def at_z(by):
        return (at(z, by) * RING + x, tp)

    def at_y(by):
        return (sp, at(y, by) * 2 + core)

    def at_sp(by):
        return (lax.rem(sp + by, 16), tp)

    partner = (sp, y * 2 + 1 - core)

    barrier = pltpu.get_barrier_semaphore()
    peers = [partner, at_sp(1), at_sp(15)]
    for by in (1, 3):
        peers.append(at_y(by))
    for by in (1, 2, 3):
        peers += [at_x(by), at_z(by)]
    for peer in peers:
        pl.semaphore_signal(barrier, inc=1, device_id=peer, device_id_type=MESH)

    def feature_cols(y_index, core_index):
        return pl.ds(pl.multiple_of((y_index * 2 + core_index) * FEATURES, FEATURES), FEATURES)

    my_cols = feature_cols(y, core)
    loads = [pltpu.make_async_copy(tokens, whole.at[:, my_cols], load_sem.at[0])]
    for number, ref in enumerate((wq, wk, wv)):
        loads.append(pltpu.make_async_copy(ref, weight.at[:, number * COLS : (number + 1) * COLS], load_sem.at[1 + number]))
    loads.append(pltpu.make_async_copy(out_grad, upstream, load_sem.at[4]))
    for load in loads:
        load.start()

    lane = lax.broadcasted_iota(jnp.int32, (8, ROUND), 1)
    row = lax.broadcasted_iota(jnp.int32, (SPAN, TILE), 0)
    column = lax.broadcasted_iota(jnp.int32, (SPAN, TILE), 1)
    low = jnp.where(column >= SEGMENT, SEGMENT, 0)
    seen = (row >= low) & (row < low + REACH + SEGMENT)
    for h in range(HEADS):
        entries = jnp.broadcast_to(table[h : h + 1, :], (8, TABLE))
        padded = jnp.concatenate([entries, jnp.zeros((8, ROUND - TABLE), F32)], axis=1)
        turned = pltpu.roll(padded, ROUND - TABLE + 1, 1)
        last = jnp.broadcast_to(table[h : h + 1, TABLE - 1 : TABLE], (8, ROUND))
        turned = jnp.where(lane < TILE, last, turned)
        skewed = pltpu.roll(jnp.broadcast_to(turned[0:1, :], (SPAN, ROUND)), 0, 1, stride=1, stride_axis=0)
        bias[h] = jnp.where(seen, skewed[:, :TILE], -jnp.inf)
        dsum[h] = jnp.zeros((SPAN, TILE), F32)
    dkv[...] = jnp.zeros(dkv.shape, F32)

    loads[0].wait()
    pl.semaphore_wait(barrier, len(peers))

    def rows_of(step):
        return pl.multiple_of(lax.rem(step + 4, CHUNKS) * TILE, TILE)

    def chunk_copy(rows, cols, target, send, recv):
        view = whole.at[rows, cols]
        return pltpu.make_async_remote_copy(
            src_ref=view, dst_ref=view, send_sem=send, recv_sem=recv, device_id=target, device_id_type=MESH
        )

    up, down = at_y(1), at_y(3)

    def gather_copy(step, d):
        return chunk_copy(pl.ds(rows_of(step), TILE), my_cols, (up, down)[d], gather_send.at[step, d], gather_recv.at[step, d])

    def gather_landed(step, d):
        cols = feature_cols(at(y, (3, 1)[d]), core)
        return chunk_copy(pl.ds(rows_of(step), TILE), cols, (up, down)[d], gather_send.at[step, d], gather_recv.at[step, d])

    def hop_copy(step, d):
        cols = feature_cols(at(y, (3, 1)[d]), core)
        rows = pl.ds(pl.multiple_of(rows_of(step) + d * SEGMENT, SEGMENT), SEGMENT)
        return chunk_copy(rows, cols, (up, down)[d], hop_send.at[step, d], hop_recv.at[step, d])

    def hop_landed(step, d):
        cols = feature_cols(at(y, 2), core)
        rows = pl.ds(pl.multiple_of(rows_of(step) + d * SEGMENT, SEGMENT), SEGMENT)
        return chunk_copy(rows, cols, (up, down)[d], hop_send.at[step, d], hop_recv.at[step, d])

    def core_copy(step, which):
        cols = feature_cols(at(y, (0, 3, 1, 2)[which]), core)
        return chunk_copy(pl.ds(rows_of(step), TILE), cols, partner, core_send.at[step, which], core_recv.at[step, which])

    def core_landed(step, which):
        cols = feature_cols(at(y, (0, 3, 1, 2)[which]), 1 - core)
        return chunk_copy(pl.ds(rows_of(step), TILE), cols, partner, core_send.at[step, which], core_recv.at[step, which])

    def halo_copy(step):
        return pltpu.make_async_remote_copy(
            src_ref=kv.at[pl.ds(pl.multiple_of(LENGTH + step * TILE, TILE), TILE), :],
            dst_ref=kv.at[pl.ds(pl.multiple_of(step * TILE, TILE), TILE), :],
            send_sem=halo_send.at[step],
            recv_sem=halo_recv.at[step],
            device_id=at_sp(1),
            device_id_type=MESH,
        )

    back_copy = pltpu.make_async_remote_copy(
        src_ref=back_send,
        dst_ref=back_recv,
        send_sem=back_sems.at[0],
        recv_sem=back_sems.at[1],
        device_id=at_sp(15),
        device_id_type=MESH,
    )

    edge = jnp.where(sp == 0, REACH, 0)

    def attend(tile):
        start = pl.multiple_of(tile * TILE, TILE)
        keys_at, here = pl.ds(start, SPAN), pl.ds(start, TILE)
        for h in range(HEADS):
            cols = slice(h * HEAD, (h + 1) * HEAD)
            value_cols = slice(COLS + h * HEAD, COLS + (h + 1) * HEAD)
            keys, values = kv[keys_at, cols], kv[keys_at, value_cols]
            asked, given = query[here, cols], upstream[here, cols]
            scores = dot(keys, asked, 1, 1) * FACTOR + bias[h]
            scores = jnp.where(row + start < edge, -jnp.inf, scores)
            top = jnp.max(scores, axis=0, keepdims=True)
            raised = jnp.exp(scores - top)
            weights = raised * (1.0 / jnp.sum(raised, axis=0, keepdims=True))
            prob_grad = dot(values, given, 1, 1)
            delta = jnp.sum(weights * prob_grad, axis=0, keepdims=True)
            score_grad = weights * (prob_grad - delta)
            weights_low, score_low = weights.astype(BF16), score_grad.astype(BF16)
            dsum[h] = dsum[h] + score_grad
            dkv[keys_at, value_cols] = dkv[keys_at, value_cols] + dot(weights_low, given)
            dkv[keys_at, cols] = dkv[keys_at, cols] + dot(score_low, asked)
            query_grad = dot(score_low, keys, 0, 0) * FACTOR
            grads[here, cols] = query_grad.astype(BF16)
            grads_t[cols, here] = query_grad.T.astype(BF16)

    for step in range(2):
        for d in range(2):
            gather_copy(step, d).start()
        core_copy(step, 0).start()
    for load in loads[1:]:
        load.wait()

    def gather_step(s, carry):
        @pl.when(s < CHUNKS)
        def _():
            for d in range(2):
                gather_landed(s, d).wait_recv()
                hop_copy(s, d).start()
            for d in range(2):
                core_copy(s, 1 + d).start()

        @pl.when(s < CHUNKS - 2)
        def _():
            for d in range(2):
                gather_copy(s + 2, d).start()
            core_copy(s + 2, 0).start()

        @pl.when((s >= 1) & (s <= CHUNKS))
        def _():
            for d in range(2):
                hop_landed(s - 1, d).wait_recv()
            core_copy(s - 1, 3).start()

        @pl.when(s == 4)
        def _():
            for step in range(2):
                halo_copy(step).wait_recv()

        @pl.when(s >= 4)
        def _():
            attend(s - 4)

        @pl.when(s == 5)
        def _():
            back_send[...] = dkv[0:REACH, :].astype(BF16)
            back_copy.start()

        @pl.when((s >= 1) & (s <= CHUNKS))
        def _():
            for which in range(4):
                core_landed(s - 1, which).wait_recv()
            start = rows_of(s - 1)
            projected = dot(whole[pl.ds(start, TILE), :], weight[...]).astype(BF16)
            query[pl.ds(start, TILE), :] = projected[:, :COLS]
            kv[pl.ds(pl.multiple_of(start + REACH, TILE), TILE), :] = projected[:, COLS:]

        @pl.when((s >= 1) & (s <= 2))
        def _():
            halo_copy(s - 1).start()

        return carry

    lax.fori_loop(0, CHUNKS + 4, gather_step, 0)

    back_copy.wait_recv()
    dkv[LENGTH:, :] = dkv[LENGTH:, :] + back_recv[...].astype(F32)

    def finish_chunk(chunk, carry):
        start = pl.multiple_of(chunk * TILE, TILE)
        total = dkv[pl.ds(pl.multiple_of(start + REACH, TILE), TILE), :]
        total = jnp.concatenate([total[:, :COLS] * FACTOR, total[:, COLS:]], axis=1)
        grads[pl.ds(start, TILE), COLS:] = total.astype(BF16)
        grads_t[COLS:, pl.ds(start, TILE)] = total.T.astype(BF16)
        return carry

    lax.fori_loop(0, CHUNKS, finish_chunk, 0)

    def first_ring(p, side):
        me = (x, z)[side]
        part = (part_a, part_b)[side]
        at_side = (at_x, at_z)[side]
        return Ring(
            me, at_side(1), at_side(3),
            lambda k, half: part.at[p, k, pl.ds(2 * half, 2)],
            lambda d: far_ab.at[p, side, d],
            lambda d: near_ab.at[p, side, d],
            lambda d: join_ab.at[p, side, d],
            (lambda kind, d: ring_ss.at[p, side, 0, kind, d], lambda kind, d: ring_rs.at[p, side, 0, kind, d]),
        )

    def second_ring(p, side):
        me = (z, x)[side]
        at_side = (at_z, at_x)[side]
        return Ring(
            me, at_side(1), at_side(3),
            lambda k, half: second_ab.at[p, side, k, half * SEGMENT : (half + 1) * SEGMENT],
            lambda d: far2_ab.at[p, side, d],
            lambda d: near2_ab.at[p, side, d],
            lambda d: join2_ab.at[p, side, d],
            (lambda kind, d: ring_ss.at[p, side, 1, kind, d], lambda kind, d: ring_rs.at[p, side, 1, kind, d]),
        )

    y_ring = Ring(
        y, up, down,
        lambda k, half: term_own.at[k, half * (LENGTH // 2) : (half + 1) * (LENGTH // 2)],
        lambda d: far_y.at[d],
        lambda d: near_y.at[d],
        lambda d: join_y.at[d],
        (lambda kind, d: y_ss.at[kind, d], lambda kind, d: y_rs.at[kind, d]),
    )

    def term(y_index, core_index):
        start = pl.multiple_of((y_index * 2 + core_index) * FEATURES, FEATURES)
        return dot(grads[...], weight[pl.ds(start, FEATURES), :], 1, 1)

    def term_copy(k):
        return pltpu.make_async_remote_copy(
            src_ref=term_send.at[k],
            dst_ref=term_recv.at[k],
            send_sem=term_ss.at[k],
            recv_sem=term_rs.at[k],
            device_id=partner,
            device_id_type=MESH,
        )

    def reduce_step(k, carry):
        @pl.when(k < 3)
        def _():
            def weight_rows(z_index, inner):
                left = grads_t[pl.ds(pl.multiple_of(k * COLS, COLS), COLS), :]
                features = pl.ds(pl.multiple_of(z_index * RING * COLS, RING * COLS), RING * COLS)
                made = dot(left, whole[:, features]).astype(BF16)
                for x_index in range(RING):
                    cut = slice(x_index * COLS, (x_index + 1) * COLS)
                    part_a[k, x_index, z_index] = made[:HEAD, cut]
                    part_b[k, z_index, x_index] = made[HEAD:, cut]
                return inner

            lax.fori_loop(0, RING, weight_rows, 0)
            rings = [first_ring(k, side) for side in range(2)]
            for ring in rings:
                ring.start_far()
            for ring in rings:
                for d in range(2):
                    ring.start_near(d)

        ahead = jnp.where(k == 0, 2, jnp.where(k == 1, 1, jnp.where(k == 2, 3, 0)))
        y_index = at(y, ahead)
        term_send[k] = term(y_index, 1 - core).astype(BF16)
        term_copy(k).start()
        made = term(y_index, core)
        term_copy(k).wait_recv()
        term_own[y_index] = (made + term_recv[k].astype(F32)).astype(BF16)

        @pl.when(k == 0)
        def _():
            y_ring.start_far()

        for d in range(2):
            @pl.when(k == 1 + d)
            def _():
                y_ring.start_near(d)

        @pl.when((k >= 1) & (k < 3))
        def _():
            for side in range(2):
                first_ring(k - 1, side).join()

        return carry

    lax.fori_loop(0, RING, reduce_step, 0)

    bias_x[x] = jnp.zeros((8, ROUND), F32)
    for h in range(HEADS):
        wide = jnp.concatenate([dsum[h], jnp.zeros((SPAN, ROUND - TILE), F32)], axis=1)
        rows = SPAN
        while rows > 24:
            rows //= 2
            wide = wide[:rows] + pltpu.roll(wide[rows:], ROUND - rows, 1)
        wide = wide[0:8] + pltpu.roll(wide[8:16], ROUND - 8, 1) + pltpu.roll(wide[16:24], ROUND - 16, 1)
        sums = wide[0:1]
        for r in range(1, 8):
            sums = sums + pltpu.roll(wide[r : r + 1], ROUND - r, 1)
        first = lax.broadcasted_iota(jnp.int32, (1, ROUND), 1)
        clipped = jnp.sum(jnp.where(first < TILE, sums, 0.0), axis=1, keepdims=True)
        placed = pltpu.roll(sums, TABLE - 1, 1)
        bias_x[x, h : h + 1, :] = jnp.where(first == TABLE - 1, clipped, placed)

    def bias_copy(buffer, me, target, send, recv, slot):
        view = buffer.at[me]
        return pltpu.make_async_remote_copy(
            src_ref=view, dst_ref=view, send_sem=send.at[slot], recv_sem=recv.at[slot], device_id=target, device_id_type=MESH
        )

    for by in (1, 2, 3):
        bias_copy(bias_x, x, at_x(by), bx_s, bx_r, by - 1).start()

    y_ring.join()
    for side in range(2):
        first_ring(2, side).join()

    for by in (1, 2, 3):
        bias_copy(bias_x, at(x, 4 - by), at_x(by), bx_s, bx_r, by - 1).wait_recv()
    bias_z[z] = (bias_x[0] + bias_x[1]) + (bias_x[2] + bias_x[3])
    for by in (1, 2, 3):
        bias_copy(bias_z, z, at_z(by), bz_s, bz_r, by - 1).start()

    def second_start(p):
        for side in range(2):
            ring = first_ring(p, side)
            for half in range(2):
                second_ab[p, side, 2 * half : 2 * half + 2] = ring.half(half).astype(BF16)
        rings = [second_ring(p, side) for side in range(2)]
        for ring in rings:
            ring.start_far()
        for ring in rings:
            for d in range(2):
                ring.start_near(d)

    def second_join(p):
        for side in range(2):
            second_ring(p, side).join()

    def second_finish(p):
        for side in range(2):
            ring = second_ring(p, side)
            total = jnp.concatenate([ring.half(0), ring.half(1)], axis=0)
            weight_stage[p, :, side * HEAD : (side + 1) * HEAD] = total.T
        pltpu.make_async_copy(weight_stage.at[p], (wq_out, wk_out, wv_out)[p], store_sem.at[p]).start()

    second_start(0)
    second_start(1)
    second_join(0)
    second_finish(0)
    second_start(2)
    second_join(1)
    second_finish(1)
    for d in range(2):
        input_stage[d * (LENGTH // 2) : (d + 1) * (LENGTH // 2), :] = y_ring.half(d).astype(BF16)
    input_store = pltpu.make_async_copy(input_stage, input_out, store_sem.at[3])
    input_store.start()
    second_join(2)
    for by in (1, 2, 3):
        bias_copy(bias_z, at(z, 4 - by), at_z(by), bz_s, bz_r, by - 1).wait_recv()
    bias_out[...] = ((bias_z[0] + bias_z[1]) + (bias_z[2] + bias_z[3]))[:HEADS, :TABLE]
    second_finish(2)

    for step in range(CHUNKS):
        for d in range(2):
            gather_copy(step, d).wait_send()
            hop_copy(step, d).wait_send()
        for which in range(4):
            core_copy(step, which).wait_send()
    for step in range(2):
        halo_copy(step).wait_send()
    back_copy.wait_send()
    for k in range(RING):
        term_copy(k).wait_send()
    y_ring.wait_sends()
    for p in range(3):
        for side in range(2):
            first_ring(p, side).wait_sends()
            second_ring(p, side).wait_sends()
    for by in (1, 2, 3):
        bias_copy(bias_x, x, at_x(by), bx_s, bx_r, by - 1).wait_send()
        bias_copy(bias_z, z, at_z(by), bz_s, bz_r, by - 1).wait_send()
    for p in range(3):
        pltpu.make_async_copy(weight_stage.at[p], (wq_out, wk_out, wv_out)[p], store_sem.at[p]).wait()
    input_store.wait()


def shards(tokens, query_weight, key_weight, value_weight, position_bias, out_grad):
    anywhere = pl.BlockSpec(memory_space=pl.ANY)
    near = pl.BlockSpec(memory_space=pltpu.VMEM)
    dma = pltpu.SemaphoreType.DMA
    vmem = pltpu.VMEM
    grad = jax.ShapeDtypeStruct((COLS, COLS), F32)
    return pl.pallas_call(
        kernel,
        name="segment_attention_grads",
        out_shape=(
            jax.ShapeDtypeStruct((LENGTH, FEATURES), BF16), grad, grad, grad,
            jax.ShapeDtypeStruct((HEADS, TABLE), F32),
        ),
        in_specs=[anywhere, anywhere, anywhere, anywhere, near, anywhere],
        out_specs=(anywhere, anywhere, anywhere, anywhere, near),
        scratch_shapes=[
            vmem((LENGTH, WIDTH), BF16),
            vmem((WIDTH, 3 * COLS), BF16),
            vmem((LENGTH, COLS), BF16),
            vmem((REACH + LENGTH, 2 * COLS), BF16),
            vmem((LENGTH, COLS), BF16),
            vmem((REACH + LENGTH, 2 * COLS), F32),
            vmem((LENGTH, 3 * COLS), BF16),
            vmem((3 * COLS, LENGTH), BF16),
            vmem((REACH, 2 * COLS), BF16),
            vmem((REACH, 2 * COLS), BF16),
            vmem((3, RING, RING, HEAD, COLS), BF16),
            vmem((3, RING, RING, HEAD, COLS), BF16),
            vmem((3, 2, 2, 2, HEAD, COLS), BF16),
            vmem((3, 2, 2, 2, HEAD, COLS), BF16),
            vmem((3, 2, 2, 2, HEAD, COLS), BF16),
            vmem((3, 2, RING, HEAD, COLS), BF16),
            vmem((3, 2, 2, SEGMENT, COLS), BF16),
            vmem((3, 2, 2, SEGMENT, COLS), BF16),
            vmem((3, 2, 2, SEGMENT, COLS), BF16),
            vmem((RING, LENGTH, FEATURES), BF16),
            vmem((RING, LENGTH, FEATURES), BF16),
            vmem((RING, LENGTH, FEATURES), BF16),
            vmem((2, LENGTH // 2, FEATURES), BF16),
            vmem((2, LENGTH // 2, FEATURES), BF16),
            vmem((2, LENGTH // 2, FEATURES), BF16),
            vmem((LENGTH, FEATURES), BF16),
            vmem((3, COLS, COLS), F32),
            vmem((HEADS, SPAN, TILE), F32),
            vmem((HEADS, SPAN, TILE), F32),
            vmem((RING, 8, ROUND), F32),
            vmem((RING, 8, ROUND), F32),
            dma((5,)),
            dma((CHUNKS, 2)), dma((CHUNKS, 2)),
            dma((CHUNKS, 2)), dma((CHUNKS, 2)),
            dma((CHUNKS, 4)), dma((CHUNKS, 4)),
            dma((2,)), dma((2,)),
            dma((2,)),
            dma((RING,)), dma((RING,)),
            dma((3, 2, 2, 3, 2)), dma((3, 2, 2, 3, 2)),
            dma((3, 2)), dma((3, 2)),
            dma((3,)), dma((3,)), dma((3,)), dma((3,)),
            dma((4,)),
        ],
        compiler_params=pltpu.CompilerParams(
            collective_id=0, has_side_effects=True, vmem_limit_bytes=67_000_000
        ),
    )(tokens, query_weight, key_weight, value_weight, position_bias, out_grad)


def solution(mesh):
    return jax.shard_map(
        shards,
        mesh=mesh,
        in_specs=(P("sp", "tp"), P(None, "tp"), P(None, "tp"), P(None, "tp"), P("tp", None), P("sp", "tp")),
        out_specs=(P("sp", "tp"), P("sp", "tp"), P("sp", "tp"), P("sp", "tp"), P("tp", None)),
        check_vma=False,
    )
```

profile of v0, /device:TPU:1, one launch (start us, length us, event | category | flops | bytes accessed | tf_op | source)
XLA Modules:
  0.0 98.7 jit_solution(17287252305640540767)
XLA Ops:
  0.6 92.2 %segment_attention_grads.1 = (bf16[768,512]{1,0:T(8,128)(2,1)}, f32[256,256]{1,0:T(8,128)}, f32[256,256]{1,0:T(8,128)}, f32[256,256]{1,0:T(8,128)}, f32[2,320]{1,0:T(2,128)}) custom-call(bf16[768,512]{1,0:T(8,128)(2,1)} %tokens.1, bf16[4096,256]{1,0:T(8,128)(2,1)} %wq.1, bf16[4096,256]{1,0:T(8,128)(2,1)} %wk.1, bf16[4096,256]{1,0:T(8,128)(2,1)} %wv.1, ...), custom_call_target="tpu_custom_call" | custom-call | tf_op jit(solution)/shard_map/segment_attention_grads/pallas_call | solution.py:497
  92.9 0.0 copy-start.1
  92.9 0.0 copy-start
  92.9 0.0 copy-start.2
  92.9 2.1 %copy.16 = bf16[768,512]{1,0:T(8,128)(2,1)} copy(bf16[768,512]{1,0:T(8,128)(2,1)} %get-tuple-element.10) | data formatting | bytes 1572864
  95.0 1.7 %copy.17 = f32[256,256]{1,0:T(8,128)} copy(f32[256,256]{1,0:T(8,128)} %get-tuple-element.11) | data formatting | bytes 524288
  96.7 0.0 copy-done.1
  96.7 0.7 copy.18
  97.4 0.0 copy-done
  97.4 0.7 copy.19
  98.1 0.0 copy-done.2
  98.1 0.6 copy.20
Async XLA Ops:
  92.9 3.8 %copy-start.1 = (f32[256,256]{1,0:T(8,128)S(1)}, f32[256,256]{1,0:T(8,128)}, u32[]{:S(2)}) copy-start(f32[256,256]{1,0:T(8,128)} %get-tuple-element.12) | copy-start | bytes 786436
  92.9 4.5 %copy-start = (f32[256,256]{1,0:T(8,128)S(1)}, f32[256,256]{1,0:T(8,128)}, u32[]{:S(2)}) copy-start(f32[256,256]{1,0:T(8,128)} %get-tuple-element.13) | copy-start | bytes 786436
  92.9 5.2 %copy-start.2 = (f32[2,320]{1,0:T(2,128)S(1)}, f32[2,320]{1,0:T(2,128)}, u32[]{:S(2)}) copy-start(f32[2,320]{1,0:T(2,128)} %get-tuple-element.14) | copy-start | bytes 7684
where the time goes:
time: 99.4 us; the launch traced here: 98.7 us
  Pallas kernels  92.2 us (93%)
  local copies, waits for them, and re-layouts  5.78 us (6%)
    pallas_call x1, Pallas kernels, shards(): pl.pallas_call(kernel, name='segment_attention_grads', out_shape=(jax.Sha...  92.2 us
    unnamed x11, local copies, waits for them, and re-layouts  5.78 us

commit v1 on v0

v1 whole, which is shorter than its diff:
```python
import functools

import jax
import jax.numpy as jnp
from jax import lax
from jax.experimental import pallas as pl
from jax.experimental.pallas import tpu as pltpu
from jax.sharding import PartitionSpec as P

MESH = pl.DeviceIdType.MESH
BF16, F32 = jnp.bfloat16, jnp.float32
SEGMENT, REACH, CLIP, HEAD = 64, 256, 256, 128
TILE = 128
SPAN = REACH + TILE
LENGTH, WIDTH, FEATURES = 768, 4096, 512
CHUNKS = LENGTH // TILE
HEADS = 2
COLS = HEADS * HEAD
FACTOR = HEAD ** (-0.5)
RING = 4
TABLE = 320
ROUND = 512


def dot(left, right, left_dim=1, right_dim=0):
    return lax.dot_general(left, right, (((left_dim,), (right_dim,)), ((), ())), preferred_element_type=F32)


class Ring:
    def __init__(self, me, up, down, block, via, direct, joined, sent, far_sem, rest_sem):
        self.near = (lax.rem(me + 1, RING), lax.rem(me + RING - 1, RING))
        self.far = lax.rem(me + 2, RING)
        self.me, self.devices, self.block = me, (up, down), block
        self.landing = (via, direct, joined)
        self.sent, self.arrived = sent, (far_sem, rest_sem, rest_sem)

    def start(self, kind, d):
        source = (self.block(self.far, d), self.block(self.near[d], 1 - d), self.block(self.near[d], d))[kind]
        pltpu.make_async_remote_copy(
            src_ref=source,
            dst_ref=self.landing[kind](d),
            send_sem=self.sent,
            recv_sem=self.arrived[kind],
            device_id=self.devices[d],
            device_id_type=MESH,
        ).start()

    def start_far(self):
        for d in range(2):
            self.start(0, d)

    def start_near(self, d):
        self.start(1, d)

    def join(self):
        for d in range(2):
            ref = self.block(self.near[d], d)
            ref[...] = (ref[...].astype(F32) + self.landing[0](d)[...].astype(F32)).astype(BF16)
            self.start(2, d)

    def half(self, d):
        total = self.block(self.me, d)[...].astype(F32) + self.landing[2](d)[...].astype(F32)
        return total + self.landing[1](1 - d)[...].astype(F32)


def await_bytes(view, sem):
    pltpu.make_async_copy(view, view, sem).wait()


def kernel(
    tokens, wq, wk, wv, table, out_grad,
    input_out, wq_out, wk_out, wv_out, bias_out,
    whole, weight, query, kv, upstream, dkv, grads, grads_t, back_send, back_recv,
    part_a, part_b, far_ab, near_join, second_ab, far2_ab, near_join2,
    term_own, term_send, term_recv, far_y, near_join_y,
    bias, dsum, bias_x, bias_z,
    load_sem, gather_recv, hop_recv, core_recv, halo_recv, term_rs, ring_rs, second_rs, y_rs, bias_rs, sent,
):
    sp, tp = lax.axis_index("sp"), lax.axis_index("tp")
    z, x = sp // RING, lax.rem(sp, RING)
    y, core = tp // 2, lax.rem(tp, 2)

    def at(value, by):
        return lax.rem(value + by, RING)

    def at_x(by):
        return (z * RING + at(x, by), tp)

    def at_z(by):
        return (at(z, by) * RING + x, tp)

    def at_y(by):
        return (sp, at(y, by) * 2 + core)

    def at_sp(by):
        return (lax.rem(sp + by, 16), tp)

    partner = (sp, y * 2 + 1 - core)

    barrier = pltpu.get_barrier_semaphore()
    peers = [partner, at_sp(1), at_sp(15)]
    for by in (1, 3):
        peers.append(at_y(by))
    for by in (1, 2, 3):
        peers += [at_x(by), at_z(by)]
    for peer in peers:
        pl.semaphore_signal(barrier, inc=1, device_id=peer, device_id_type=MESH)

    def feature_cols(y_index, core_index):
        return pl.ds(pl.multiple_of((y_index * 2 + core_index) * FEATURES, FEATURES), FEATURES)

    my_cols = feature_cols(y, core)
    own_load = pltpu.make_async_copy(tokens, whole.at[:, my_cols], load_sem.at[0])
    own_load.start()
    with jax.named_scope("entry"):
        own_load.wait()
        pl.semaphore_wait(barrier, len(peers))

    def rows_of(step):
        return pl.multiple_of(lax.rem(step + 4, CHUNKS) * TILE, TILE)

    def chunk_copy(rows, cols, target, send, recv):
        view = whole.at[rows, cols]
        return pltpu.make_async_remote_copy(
            src_ref=view, dst_ref=view, send_sem=send, recv_sem=recv, device_id=target, device_id_type=MESH
        )

    up, down = at_y(1), at_y(3)

    def gather_copy(step, d):
        return chunk_copy(pl.ds(rows_of(step), TILE), my_cols, (up, down)[d], sent.at[0], gather_recv.at[step])

    def hop_copy(step, d):
        cols = feature_cols(at(y, (3, 1)[d]), core)
        rows = pl.ds(pl.multiple_of(rows_of(step) + d * SEGMENT, SEGMENT), SEGMENT)
        return chunk_copy(rows, cols, (up, down)[d], sent.at[1], hop_recv.at[step])

    def core_copy(step, which):
        cols = feature_cols(at(y, (0, 3, 1, 2)[which]), core)
        return chunk_copy(pl.ds(rows_of(step), TILE), cols, partner, sent.at[2], core_recv.at[step])

    def halo_copy(step):
        return pltpu.make_async_remote_copy(
            src_ref=kv.at[pl.ds(pl.multiple_of(LENGTH + step * TILE, TILE), TILE), :],
            dst_ref=kv.at[pl.ds(pl.multiple_of(step * TILE, TILE), TILE), :],
            send_sem=sent.at[3],
            recv_sem=halo_recv.at[0],
            device_id=at_sp(1),
            device_id_type=MESH,
        )

    back_copy = pltpu.make_async_remote_copy(
        src_ref=back_send,
        dst_ref=back_recv,
        send_sem=sent.at[4],
        recv_sem=halo_recv.at[1],
        device_id=at_sp(15),
        device_id_type=MESH,
    )

    edge = jnp.where(sp == 0, REACH, 0)
    row = lax.broadcasted_iota(jnp.int32, (SPAN, TILE), 0)

    def attend(tile):
        start = pl.multiple_of(tile * TILE, TILE)
        keys_at, here = pl.ds(start, SPAN), pl.ds(start, TILE)
        heads = []
        for h in range(HEADS):
            cols = slice(h * HEAD, (h + 1) * HEAD)
            value_cols = slice(COLS + h * HEAD, COLS + (h + 1) * HEAD)
            keys, values = kv[keys_at, cols], kv[keys_at, value_cols]
            asked, given = query[here, cols], upstream[here, cols]
            heads.append((cols, value_cols, keys, asked, given, dot(keys, asked, 1, 1), dot(values, given, 1, 1)))
        lows = []
        for h in range(HEADS):
            scores = heads[h][5] * FACTOR + bias[h]
            scores = jnp.where(row + start < edge, -jnp.inf, scores)
            top = jnp.max(scores, axis=0, keepdims=True)
            raised = jnp.exp(scores - top)
            weights = raised * (1.0 / jnp.sum(raised, axis=0, keepdims=True))
            prob_grad = heads[h][6]
            delta = jnp.sum(weights * prob_grad, axis=0, keepdims=True)
            score_grad = weights * (prob_grad - delta)
            dsum[h] = dsum[h] + score_grad
            lows.append((weights.astype(BF16), score_grad.astype(BF16)))
        for h in range(HEADS):
            cols, value_cols, keys, asked, given = heads[h][:5]
            weights_low, score_low = lows[h]
            dkv[keys_at, value_cols] = dkv[keys_at, value_cols] + dot(weights_low, given)
            dkv[keys_at, cols] = dkv[keys_at, cols] + dot(score_low, asked)
            query_grad = dot(score_low, keys, 0, 0) * FACTOR
            grads[here, cols] = query_grad.astype(BF16)
            grads_t[cols, here] = query_grad.T.astype(BF16)

    for step in range(2):
        for d in range(2):
            gather_copy(step, d).start()
        core_copy(step, 0).start()

    loads = []
    for number, ref in enumerate((wq, wk, wv)):
        loads.append(pltpu.make_async_copy(ref, weight.at[:, number * COLS : (number + 1) * COLS], load_sem.at[1 + number]))
    loads.append(pltpu.make_async_copy(out_grad, upstream, load_sem.at[4]))
    for load in loads:
        load.start()

    lane = lax.broadcasted_iota(jnp.int32, (8, ROUND), 1)
    column = lax.broadcasted_iota(jnp.int32, (SPAN, TILE), 1)
    low = jnp.where(column >= SEGMENT, SEGMENT, 0)
    seen = (row >= low) & (row < low + REACH + SEGMENT)
    for h in range(HEADS):
        entries = jnp.broadcast_to(table[h : h + 1, :], (8, TABLE))
        padded = jnp.concatenate([entries, jnp.zeros((8, ROUND - TABLE), F32)], axis=1)
        turned = pltpu.roll(padded, ROUND - TABLE + 1, 1)
        last = jnp.broadcast_to(table[h : h + 1, TABLE - 1 : TABLE], (8, ROUND))
        turned = jnp.where(lane < TILE, last, turned)
        skewed = pltpu.roll(jnp.broadcast_to(turned[0:1, :], (SPAN, ROUND)), 0, 1, stride=1, stride_axis=0)
        bias[h] = jnp.where(seen, skewed[:, :TILE], -jnp.inf)
        dsum[h] = jnp.zeros((SPAN, TILE), F32)
    dkv[...] = jnp.zeros(dkv.shape, F32)

    for load in loads:
        load.wait()

    def gather_step(s, carry):
        @pl.when(s < CHUNKS)
        def _():
            with jax.named_scope("gather_wait"):
                await_bytes(whole.at[0 : 2 * TILE, 0:FEATURES], gather_recv.at[s])
                for d in range(2):
                    hop_copy(s, d).start()
                for d in range(2):
                    core_copy(s, 1 + d).start()

        @pl.when(s < CHUNKS - 2)
        def _():
            for d in range(2):
                gather_copy(s + 2, d).start()
            core_copy(s + 2, 0).start()

        @pl.when((s >= 1) & (s <= CHUNKS))
        def _():
            with jax.named_scope("hop_wait"):
                await_bytes(whole.at[0:TILE, 0:FEATURES], hop_recv.at[s - 1])
                core_copy(s - 1, 3).start()

        @pl.when(s == 4)
        def _():
            with jax.named_scope("halo_wait"):
                await_bytes(kv.at[0:REACH, :], halo_recv.at[0])

        @pl.when(s >= 4)
        def _():
            with jax.named_scope("attend"):
                attend(s - 4)

        @pl.when(s == 5)
        def _():
            back_send[...] = dkv[0:REACH, :].astype(BF16)
            back_copy.start()

        @pl.when((s >= 1) & (s <= CHUNKS))
        def _():
            with jax.named_scope("core_wait"):
                await_bytes(whole.at[0:TILE, 0 : 4 * FEATURES], core_recv.at[s - 1])

            with jax.named_scope("project"):
                start = rows_of(s - 1)
                projected = dot(whole[pl.ds(start, TILE), :], weight[...]).astype(BF16)
                query[pl.ds(start, TILE), :] = projected[:, :COLS]
                kv[pl.ds(pl.multiple_of(start + REACH, TILE), TILE), :] = projected[:, COLS:]

        @pl.when((s >= 1) & (s <= 2))
        def _():
            halo_copy(s - 1).start()

        return carry

    lax.fori_loop(0, CHUNKS + 4, gather_step, 0)

    def first_ring(p, side):
        me = (x, z)[side]
        part = (part_a, part_b)[side]
        at_side = (at_x, at_z)[side]
        return Ring(
            me, at_side(1), at_side(3),
            lambda k, half: part.at[p, k, pl.ds(2 * half, 2)],
            lambda d: far_ab.at[p, side, d],
            lambda d: near_join.at[p, 0, side, d],
            lambda d: near_join.at[p, 1, side, d],
            sent.at[5], ring_rs.at[p, 0], ring_rs.at[p, 1],
        )

    def second_ring(p, side):
        me = (z, x)[side]
        at_side = (at_z, at_x)[side]
        return Ring(
            me, at_side(1), at_side(3),
            lambda k, half: second_ab.at[p, side, k, half * SEGMENT : (half + 1) * SEGMENT],
            lambda d: far2_ab.at[p, side, d],
            lambda d: near_join2.at[p, 0, side, d],
            lambda d: near_join2.at[p, 1, side, d],
            sent.at[6], second_rs.at[p, 0], second_rs.at[p, 1],
        )

    y_ring = Ring(
        y, up, down,
        lambda k, half: term_own.at[k, half * (LENGTH // 2) : (half + 1) * (LENGTH // 2)],
        lambda d: far_y.at[d],
        lambda d: near_join_y.at[0, d],
        lambda d: near_join_y.at[1, d],
        sent.at[7], y_rs.at[0], y_rs.at[1],
    )

    def term(y_index, core_index):
        start = pl.multiple_of((y_index * 2 + core_index) * FEATURES, FEATURES)
        return dot(grads[...], weight[pl.ds(start, FEATURES), :], 1, 1)

    def term_copy(k):
        return pltpu.make_async_remote_copy(
            src_ref=term_send.at[k],
            dst_ref=term_recv.at[k],
            send_sem=sent.at[8],
            recv_sem=term_rs.at[k],
            device_id=partner,
            device_id_type=MESH,
        )

    def send_term(k):
        with jax.named_scope("term_send"):
            term_send[k] = term(at(y, ahead(k)), 1 - core).astype(BF16)
        term_copy(k).start()

    def ahead(k):
        return jnp.where(k == 0, 2, jnp.where(k == 1, 1, jnp.where(k == 2, 3, 0)))

    def bias_send(buffer, me, targets, which):
        view = buffer.at[me]
        for target in targets:
            pltpu.make_async_remote_copy(
                src_ref=view, dst_ref=view, send_sem=sent.at[9], recv_sem=bias_rs.at[which], device_id=target, device_id_type=MESH
            ).start()

    def bias_sums():
        bias_x[x] = jnp.zeros((8, ROUND), F32)
        for h in range(HEADS):
            wide = jnp.concatenate([dsum[h], jnp.zeros((SPAN, ROUND - TILE), F32)], axis=1)
            rows = SPAN
            while rows > 24:
                rows //= 2
                wide = wide[:rows] + pltpu.roll(wide[rows:], ROUND - rows, 1)
            wide = wide[0:8] + pltpu.roll(wide[8:16], ROUND - 8, 1) + pltpu.roll(wide[16:24], ROUND - 16, 1)
            sums = wide[0:1]
            for r in range(1, 8):
                sums = sums + pltpu.roll(wide[r : r + 1], ROUND - r, 1)
            first = lax.broadcasted_iota(jnp.int32, (1, ROUND), 1)
            clipped = jnp.sum(jnp.where(first < TILE, sums, 0.0), axis=1, keepdims=True)
            placed = pltpu.roll(sums, TABLE - 1, 1)
            bias_x[x, h : h + 1, :] = jnp.where(first == TABLE - 1, clipped, placed)

    def finish():
        with jax.named_scope("back_wait"):
            back_copy.wait_recv()
            dkv[LENGTH:, :] = dkv[LENGTH:, :] + back_recv[...].astype(F32)

        def finish_chunk(chunk, carry):
            start = pl.multiple_of(chunk * TILE, TILE)
            total = dkv[pl.ds(pl.multiple_of(start + REACH, TILE), TILE), :]
            total = jnp.concatenate([total[:, :COLS] * FACTOR, total[:, COLS:]], axis=1)
            grads[pl.ds(start, TILE), COLS:] = total.astype(BF16)
            grads_t[COLS:, pl.ds(start, TILE)] = total.T.astype(BF16)
            return carry

        with jax.named_scope("finish"):
            lax.fori_loop(0, CHUNKS, finish_chunk, 0)

    def weight_part(k):
        def rows(i, inner):
            z_index = at(z, 2 + i)
            left = grads_t[pl.ds(pl.multiple_of(k * COLS, COLS), COLS), :]
            features = pl.ds(pl.multiple_of(z_index * RING * COLS, RING * COLS), RING * COLS)
            made = dot(left, whole[:, features]).astype(BF16)
            for x_index in range(RING):
                cut = slice(x_index * COLS, (x_index + 1) * COLS)
                part_b[k, z_index, x_index] = made[HEAD:, cut]

                @pl.when((k > 0) | (x_index != at(x, 2)))
                def _():
                    part_a[k, x_index, z_index] = made[:HEAD, cut]

            @pl.when(i == 0)
            def _():
                first_ring(k, 1).start_far()

            return inner

        with jax.named_scope("weight_rows"):
            lax.fori_loop(0, RING, rows, 0)

        @pl.when(k > 0)
        def _():
            first_ring(k, 0).start_far()

        for side in range(2):
            for d in range(2):
                first_ring(k, side).start_near(d)

    def own_term(k):
        with jax.named_scope("term_own"):
            y_index = at(y, ahead(k))
            made = term(y_index, core)
            term_copy(k).wait_recv()
            term_own[y_index] = (made + term_recv[k].astype(F32)).astype(BF16)

    with jax.named_scope("weight_first"):
        far_x = at(x, 2)
        for z_index in range(RING):
            features = pl.ds(pl.multiple_of(z_index * RING * COLS + far_x * COLS, COLS), COLS)
            part_a[0, far_x, z_index] = dot(grads_t[0:HEAD, :], whole[:, features]).astype(BF16)
        first_ring(0, 0).start_far()

    def first_join(p):
        with jax.named_scope("join_first"):
            await_bytes(far_ab.at[p], ring_rs.at[p, 0])
            for side in range(2):
                first_ring(p, side).join()

    def reduce_step(k, carry):
        @pl.when(k < 3)
        def _():
            weight_part(k)

        @pl.when(k == 0)
        def _():
            finish()
            with jax.named_scope("bias_sums"):
                bias_sums()
            bias_send(bias_x, x, [at_x(by) for by in (1, 2, 3)], 0)

        @pl.when(k >= 1)
        def _():
            own_term(k - 1)

        @pl.when(k == 1)
        def _():
            y_ring.start_far()

        for d in range(2):
            @pl.when(k == 2 + d)
            def _():
                y_ring.start_near(d)

        @pl.when(k < RING)
        def _():
            send_term(k)

        @pl.when((k >= 1) & (k < 3))
        def _():
            first_join(k - 1)

        @pl.when(k == 3)
        def _():
            with jax.named_scope("bias_x"):
                await_bytes(bias_x.at[0:3], bias_rs.at[0])
                bias_z[z] = (bias_x[0] + bias_x[1]) + (bias_x[2] + bias_x[3])
                bias_send(bias_z, z, [at_z(by) for by in (1, 2, 3)], 1)

        return carry

    lax.fori_loop(0, RING + 1, reduce_step, 0)

    with jax.named_scope("join_y"):
        await_bytes(far_y, y_rs.at[0])
        y_ring.join()

    def second_start(p):
        with jax.named_scope(f"second_start_{p}"):
            await_bytes(near_join.at[p], ring_rs.at[p, 1])
            for side in range(2):
                ring = first_ring(p, side)
                for half in range(2):
                    second_ab[p, side, 2 * half : 2 * half + 2] = ring.half(half).astype(BF16)
            rings = [second_ring(p, side) for side in range(2)]
            for ring in rings:
                ring.start_far()
            for ring in rings:
                for d in range(2):
                    ring.start_near(d)

    def second_join(p):
        with jax.named_scope(f"second_join_{p}"):
            await_bytes(far2_ab.at[p], second_rs.at[p, 0])
            for side in range(2):
                second_ring(p, side).join()

    def second_finish(p):
        with jax.named_scope(f"second_finish_{p}"):
            await_bytes(near_join2.at[p], second_rs.at[p, 1])
            for side in range(2):
                ring = second_ring(p, side)
                total = jnp.concatenate([ring.half(0), ring.half(1)], axis=0)
                (wq_out, wk_out, wv_out)[p][:, side * HEAD : (side + 1) * HEAD] = total.T

    second_start(0)
    first_join(2)
    second_start(1)
    second_join(0)
    second_start(2)
    second_join(1)
    second_finish(0)
    with jax.named_scope("bias_z"):
        await_bytes(bias_z.at[0:3], bias_rs.at[1])
        bias_out[...] = ((bias_z[0] + bias_z[1]) + (bias_z[2] + bias_z[3]))[:HEADS, :TABLE]
    second_join(2)
    second_finish(1)
    with jax.named_scope("input_sum"):
        await_bytes(near_join_y, y_rs.at[1])
        for d in range(2):
            input_out[d * (LENGTH // 2) : (d + 1) * (LENGTH // 2), :] = y_ring.half(d).astype(BF16)
    second_finish(2)

    with jax.named_scope("drain"):
        await_bytes(whole.at[:, 0 : 2 * FEATURES], sent.at[0])
        await_bytes(whole.at[:, 0:FEATURES], sent.at[1])
        await_bytes(whole.at[:, 0 : 4 * FEATURES], sent.at[2])
        await_bytes(kv.at[0:REACH, :], sent.at[3])
        await_bytes(back_send, sent.at[4])
        await_bytes(far_ab, sent.at[5])
        await_bytes(near_join, sent.at[5])
        await_bytes(far2_ab, sent.at[6])
        await_bytes(near_join2, sent.at[6])
        await_bytes(far_y, sent.at[7])
        await_bytes(near_join_y, sent.at[7])
        await_bytes(term_recv, sent.at[8])
        await_bytes(bias_x.at[0:3], sent.at[9])
        await_bytes(bias_z.at[0:3], sent.at[9])


def shards(tokens, query_weight, key_weight, value_weight, position_bias, out_grad):
    anywhere = pl.BlockSpec(memory_space=pl.ANY)
    near = pl.BlockSpec(memory_space=pltpu.VMEM)
    dma = pltpu.SemaphoreType.DMA
    vmem = pltpu.VMEM
    grad = vmem((COLS, COLS), F32)
    return pl.pallas_call(
        kernel,
        name="segment_attention_grads",
        out_shape=(
            vmem((LENGTH, FEATURES), BF16), grad, grad, grad,
            vmem((HEADS, TABLE), F32),
        ),
        in_specs=[anywhere, anywhere, anywhere, anywhere, near, anywhere],
        out_specs=(near,) * 5,
        scratch_shapes=[
            vmem((LENGTH, WIDTH), BF16),
            vmem((WIDTH, 3 * COLS), BF16),
            vmem((LENGTH, COLS), BF16),
            vmem((REACH + LENGTH, 2 * COLS), BF16),
            vmem((LENGTH, COLS), BF16),
            vmem((REACH + LENGTH, 2 * COLS), F32),
            vmem((LENGTH, 3 * COLS), BF16),
            vmem((3 * COLS, LENGTH), BF16),
            vmem((REACH, 2 * COLS), BF16),
            vmem((REACH, 2 * COLS), BF16),
            vmem((3, RING, RING, HEAD, COLS), BF16),
            vmem((3, RING, RING, HEAD, COLS), BF16),
            vmem((3, 2, 2, 2, HEAD, COLS), BF16),
            vmem((3, 2, 2, 2, 2, HEAD, COLS), BF16),
            vmem((3, 2, RING, HEAD, COLS), BF16),
            vmem((3, 2, 2, SEGMENT, COLS), BF16),
            vmem((3, 2, 2, 2, SEGMENT, COLS), BF16),
            vmem((RING, LENGTH, FEATURES), BF16),
            vmem((RING, LENGTH, FEATURES), BF16),
            vmem((RING, LENGTH, FEATURES), BF16),
            vmem((2, LENGTH // 2, FEATURES), BF16),
            vmem((2, 2, LENGTH // 2, FEATURES), BF16),
            vmem((HEADS, SPAN, TILE), F32),
            vmem((HEADS, SPAN, TILE), F32),
            vmem((RING, 8, ROUND), F32),
            vmem((RING, 8, ROUND), F32),
            dma((5,)),
            dma((CHUNKS,)), dma((CHUNKS,)), dma((CHUNKS,)),
            dma((3,)),
            dma((RING,)),
            dma((3, 2)), dma((3, 2)), dma((2,)),
            dma((2,)),
            dma((10,)),
        ],
        compiler_params=pltpu.CompilerParams(
            collective_id=0, has_side_effects=True, vmem_limit_bytes=62_000_000
        ),
    )(tokens, query_weight, key_weight, value_weight, position_bias, out_grad)


def solution(mesh):
    return jax.shard_map(
        shards,
        mesh=mesh,
        in_specs=(P("sp", "tp"), P(None, "tp"), P(None, "tp"), P(None, "tp"), P("tp", None), P("sp", "tp")),
        out_specs=(P("sp", "tp"), P("sp", "tp"), P("sp", "tp"), P("sp", "tp"), P("tp", None)),
        check_vma=False,
    )
```

time: 99.4 us -> 85.4 us (0.86)
  Pallas kernels: 92.2 us -> 81 us
  local copies, waits for them, and re-layouts: 5.78 us -> 3.57 us
    pallas_call x1, Pallas kernels: 92.2 us -> 81 us  [shards(): pl.pallas_call(kernel, name='segment_attention_grads', out_shape=(vmem((L...]
    unnamed x11 -> x5, local copies, waits for them, and re-layouts: 5.78 us -> 3.57 us
where the time goes in v1:
time: 85.4 us; the launch traced here: 85.2 us
  Pallas kernels  81 us (95%)
  local copies, waits for them, and re-layouts  3.57 us (4%)
    pallas_call x1, Pallas kernels, shards(): pl.pallas_call(kernel, name='segment_attention_grads', out_shape=(vmem((L...  81 us
    unnamed x5, local copies, waits for them, and re-layouts  3.57 us

profile of v1, /device:TPU:1, one launch (start us, length us, event | category | flops | bytes accessed | tf_op | source)
XLA Modules:
  0.0 85.2 jit_solution(6616224774176011204)
XLA Ops:
  0.6 81.0 %segment_attention_grads.1 = (bf16[768,512]{1,0:T(8,128)(2,1)S(1)}, f32[256,256]{1,0:T(8,128)S(1)}, f32[256,256]{1,0:T(8,128)S(1)}, f32[256,256]{1,0:T(8,128)S(1)}, f32[2,320]{1,0:T(2,128)S(1)}) custom-call(bf16[768,512]{1,0:T(8,128)(2,1)} %tokens.1, bf16[4096,256]{1,0:T(8,128)(2,1)} %wq.1, bf16[4096,256]{1,0:T(8,128)(2,1)} %wk.1, bf16[4096,256]{1,0:T(8,128)(2,1)} %wv.1, ...), custom_call_target="tpu_custom_call" | custom-call | tf_op jit(solution)/shard_map/segment_attention_grads/pallas_call | solution.py:545
  81.6 0.9 %copy.16 = bf16[768,512]{1,0:T(8,128)(2,1)} copy(bf16[768,512]{1,0:T(8,128)(2,1)S(1)} %get-tuple-element.5) | data formatting | bytes 1572864
  82.5 0.6 copy.20
  83.1 0.7 copy.17
  83.8 0.7 copy.18
  84.5 0.7 copy.19

commit v2 on v1

--- a/solution.py
+++ b/solution.py
@@ -20,6 +20,7 @@
 RING = 4
 TABLE = 320
 ROUND = 512
+AHEAD = (2, 1, 3, 0)
 
 
 def dot(left, right, left_dim=1, right_dim=0):
@@ -68,13 +69,13 @@
 
 
 def kernel(
-    tokens, wq, wk, wv, table, out_grad,
+    tokens, wq, wk, wv, position_bias, out_grad,
     input_out, wq_out, wk_out, wv_out, bias_out,
-    whole, weight, query, kv, upstream, dkv, grads, grads_t, back_send, back_recv,
+    table, whole, weight, projected, query, kv, upstream, dkv, grads, grads_t, back_send, back_recv,
     part_a, part_b, far_ab, near_join, second_ab, far2_ab, near_join2,
     term_own, term_send, term_recv, far_y, near_join_y,
     bias, dsum, bias_x, bias_z,
-    load_sem, gather_recv, hop_recv, core_recv, halo_recv, term_rs, ring_rs, second_rs, y_rs, bias_rs, sent,
+    load_sem, pass_recv, gather_recv, hop_recv, core_recv, last_recv, halo_recv, term_rs, ring_rs, second_rs, y_rs, bias_rs, sent,
 ):
     sp, tp = lax.axis_index("sp"), lax.axis_index("tp")
     z, x = sp // RING, lax.rem(sp, RING)
@@ -110,10 +111,12 @@
         return pl.ds(pl.multiple_of((y_index * 2 + core_index) * FEATURES, FEATURES), FEATURES)
 
     my_cols = feature_cols(y, core)
-    own_load = pltpu.make_async_copy(tokens, whole.at[:, my_cols], load_sem.at[0])
-    own_load.start()
+    own_loads = []
+    for number, (first, last) in enumerate(((4 * TILE, 5 * TILE), (5 * TILE, 6 * TILE), (0, 4 * TILE))):
+        own = pltpu.make_async_copy(tokens.at[first:last, :], whole.at[first:last, my_cols], load_sem.at[number])
+        own.start()
+        own_loads.append(own)
     with jax.named_scope("entry"):
-        own_load.wait()
         pl.semaphore_wait(barrier, len(peers))
 
     def rows_of(step):
@@ -127,8 +130,12 @@
 
     up, down = at_y(1), at_y(3)
 
-    def gather_copy(step, d):
-        return chunk_copy(pl.ds(rows_of(step), TILE), my_cols, (up, down)[d], sent.at[0], gather_recv.at[step])
+    def gather_start(step):
+        for half in range(2):
+            for d in range(2):
+                first = pl.multiple_of(rows_of(step) + (half ^ d) * SEGMENT, SEGMENT)
+                sem = (pass_recv, gather_recv)[half].at[step]
+                chunk_copy(pl.ds(first, SEGMENT), my_cols, (up, down)[d], sent.at[0], sem).start()
 
     def hop_copy(step, d):
         cols = feature_cols(at(y, (3, 1)[d]), core)
@@ -137,7 +144,8 @@
 
     def core_copy(step, which):
         cols = feature_cols(at(y, (0, 3, 1, 2)[which]), core)
-        return chunk_copy(pl.ds(rows_of(step), TILE), cols, partner, sent.at[2], core_recv.at[step])
+        sem = (last_recv if which == 3 else core_recv).at[step]
+        return chunk_copy(pl.ds(rows_of(step), TILE), cols, partner, sent.at[2], sem)
 
     def halo_copy(step):
         return pltpu.make_async_remote_copy(
@@ -149,20 +157,23 @@
             device_id_type=MESH,
         )
 
-    back_copy = pltpu.make_async_remote_copy(
-        src_ref=back_send,
-        dst_ref=back_recv,
-        send_sem=sent.at[4],
-        recv_sem=halo_recv.at[1],
-        device_id=at_sp(15),
-        device_id_type=MESH,
-    )
+    def back_start(half):
+        rows = slice(half * TILE, (half + 1) * TILE)
+        back_send[rows] = dkv[rows, :].astype(BF16)
+        pltpu.make_async_remote_copy(
+            src_ref=back_send.at[rows],
+            dst_ref=back_recv.at[rows],
+            send_sem=sent.at[4],
+            recv_sem=halo_recv.at[1],
+            device_id=at_sp(15),
+            device_id_type=MESH,
+        ).start()
 
     edge = jnp.where(sp == 0, REACH, 0)
     row = lax.broadcasted_iota(jnp.int32, (SPAN, TILE), 0)
 
     def attend(tile):
-        start = pl.multiple_of(tile * TILE, TILE)
+        start = tile * TILE if isinstance(tile, int) else pl.multiple_of(tile * TILE, TILE)
         keys_at, here = pl.ds(start, SPAN), pl.ds(start, TILE)
         heads = []
         for h in range(HEADS):
@@ -174,7 +185,8 @@
         lows = []
         for h in range(HEADS):
             scores = heads[h][5] * FACTOR + bias[h]
-            scores = jnp.where(row + start < edge, -jnp.inf, scores)
+            if not isinstance(tile, int):
+                scores = jnp.where(row + start < edge, -jnp.inf, scores)
             top = jnp.max(scores, axis=0, keepdims=True)
             raised = jnp.exp(scores - top)
             weights = raised * (1.0 / jnp.sum(raised, axis=0, keepdims=True))
@@ -193,14 +205,17 @@
             grads_t[cols, here] = query_grad.T.astype(BF16)
 
     for step in range(2):
-        for d in range(2):
-            gather_copy(step, d).start()
+        own_loads[step].wait()
+        gather_start(step)
         core_copy(step, 0).start()
-
+    own_loads[2].wait()
+
+    table_load = pltpu.make_async_copy(position_bias, table, load_sem.at[7])
+    table_load.start()
     loads = []
     for number, ref in enumerate((wq, wk, wv)):
-        loads.append(pltpu.make_async_copy(ref, weight.at[:, number * COLS : (number + 1) * COLS], load_sem.at[1 + number]))
-    loads.append(pltpu.make_async_copy(out_grad, upstream, load_sem.at[4]))
+        loads.append(pltpu.make_async_copy(ref, weight.at[:, number * COLS : (number + 1) * COLS], load_sem.at[3 + number]))
+    loads.append(pltpu.make_async_copy(out_grad, upstream, load_sem.at[6]))
     for load in loads:
         load.start()
 
@@ -208,6 +223,7 @@
     column = lax.broadcasted_iota(jnp.int32, (SPAN, TILE), 1)
     low = jnp.where(column >= SEGMENT, SEGMENT, 0)
     seen = (row >= low) & (row < low + REACH + SEGMENT)
+    table_load.wait()
     for h in range(HEADS):
         entries = jnp.broadcast_to(table[h : h + 1, :], (8, TABLE))
         padded = jnp.concatenate([entries, jnp.zeros((8, ROUND - TABLE), F32)], axis=1)
@@ -222,61 +238,95 @@
     for load in loads:
         load.wait()
 
+    def project_from(step, blocks):
+        total = None
+        for which in blocks:
+            for on in (core, 1 - core):
+                cols = feature_cols(at(y, (0, 3, 1, 2)[which]), on)
+                part = dot(whole[pl.ds(rows_of(step), TILE), cols], weight[cols, :])
+                total = part if total is None else total + part
+        return total
+
+    def hop_landed(step):
+        with jax.named_scope("hop_wait"):
+            await_bytes(whole.at[0:TILE, 0:FEATURES], hop_recv.at[step])
+            core_copy(step, 3).start()
+
     def gather_step(s, carry):
         @pl.when(s < CHUNKS)
         def _():
-            with jax.named_scope("gather_wait"):
-                await_bytes(whole.at[0 : 2 * TILE, 0:FEATURES], gather_recv.at[s])
+            with jax.named_scope("pass_wait"):
+                await_bytes(whole.at[0:TILE, 0:FEATURES], pass_recv.at[s])
                 for d in range(2):
                     hop_copy(s, d).start()
+
+        @pl.when(s < CHUNKS - 2)
+        def _():
+            gather_start(s + 2)
+            core_copy(s + 2, 0).start()
+
+        @pl.when(s == CHUNKS)
+        def _():
+            hop_landed(s - 1)
+
+        @pl.when(s >= 1)
+        def _():
+            with jax.named_scope("core_wait"):
+                await_bytes(whole.at[0:TILE, 0 : 3 * FEATURES], core_recv.at[s - 1])
+            with jax.named_scope("project"):
+                projected[...] = project_from(s - 1, (0, 1, 2))
+
+        @pl.when(s < CHUNKS)
+        def _():
+            with jax.named_scope("gather_wait"):
+                await_bytes(whole.at[0:TILE, 0:FEATURES], gather_recv.at[s])
                 for d in range(2):
                     core_copy(s, 1 + d).start()
 
-        @pl.when(s < CHUNKS - 2)
-        def _():
-            for d in range(2):
-                gather_copy(s + 2, d).start()
-            core_copy(s + 2, 0).start()
-
-        @pl.when((s >= 1) & (s <= CHUNKS))
-        def _():
-            with jax.named_scope("hop_wait"):
-                await_bytes(whole.at[0:TILE, 0:FEATURES], hop_recv.at[s - 1])
-                core_copy(s - 1, 3).start()
+        @pl.when((s >= 1) & (s < CHUNKS))
+        def _():
+            hop_landed(s - 1)
 
         @pl.when(s == 4)
         def _():
             with jax.named_scope("halo_wait"):
                 await_bytes(kv.at[0:REACH, :], halo_recv.at[0])
 
-        @pl.when(s >= 4)
+        @pl.when((s == 4) | (s == 6))
         def _():
             with jax.named_scope("attend"):
-                attend(s - 4)
-
-        @pl.when(s == 5)
-        def _():
-            back_send[...] = dkv[0:REACH, :].astype(BF16)
-            back_copy.start()
-
-        @pl.when((s >= 1) & (s <= CHUNKS))
-        def _():
-            with jax.named_scope("core_wait"):
-                await_bytes(whole.at[0:TILE, 0 : 4 * FEATURES], core_recv.at[s - 1])
-
-            with jax.named_scope("project"):
+                attend(jnp.where(s == 4, 0, 2))
+
+            @pl.when(s == 4)
+            def _():
+                back_start(0)
+
+        @pl.when(s >= 1)
+        def _():
+            with jax.named_scope("last_wait"):
+                await_bytes(whole.at[0:TILE, 0:FEATURES], last_recv.at[s - 1])
+            with jax.named_scope("project_rest"):
                 start = rows_of(s - 1)
-                projected = dot(whole[pl.ds(start, TILE), :], weight[...]).astype(BF16)
-                query[pl.ds(start, TILE), :] = projected[:, :COLS]
-                kv[pl.ds(pl.multiple_of(start + REACH, TILE), TILE), :] = projected[:, COLS:]
+                low = (projected[...] + project_from(s - 1, (3,))).astype(BF16)
+                query[pl.ds(start, TILE), :] = low[:, :COLS]
+                kv[pl.ds(pl.multiple_of(start + REACH, TILE), TILE), :] = low[:, COLS:]
 
         @pl.when((s >= 1) & (s <= 2))
         def _():
             halo_copy(s - 1).start()
 
+        @pl.when(s == 4)
+        def _():
+            with jax.named_scope("attend"):
+                attend(s - 3)
+            back_start(1)
+
         return carry
 
-    lax.fori_loop(0, CHUNKS + 4, gather_step, 0)
+    lax.fori_loop(0, CHUNKS + 1, gather_step, 0)
+    with jax.named_scope("attend_last"):
+        for tile in range(3, CHUNKS):
+            attend(tile)
 
     def first_ring(p, side):
         me = (x, z)[side]
@@ -312,27 +362,30 @@
         sent.at[7], y_rs.at[0], y_rs.at[1],
     )
 
-    def term(y_index, core_index):
+    halves = (slice(0, LENGTH // 2), slice(LENGTH // 2, LENGTH))
+
+    def term(y_index, core_index, rows):
         start = pl.multiple_of((y_index * 2 + core_index) * FEATURES, FEATURES)
-        return dot(grads[...], weight[pl.ds(start, FEATURES), :], 1, 1)
-
-    def term_copy(k):
-        return pltpu.make_async_remote_copy(
-            src_ref=term_send.at[k],
-            dst_ref=term_recv.at[k],
+        return dot(grads[rows, :], weight[pl.ds(start, FEATURES), :], 1, 1)
+
+    def send_term(k, rows, sem):
+        with jax.named_scope("term_send"):
+            term_send[k, rows] = term(at(y, AHEAD[k]), 1 - core, rows).astype(BF16)
+        pltpu.make_async_remote_copy(
+            src_ref=term_send.at[k, rows],
+            dst_ref=term_recv.at[k, rows],
             send_sem=sent.at[8],
-            recv_sem=term_rs.at[k],
+            recv_sem=term_rs.at[sem],
             device_id=partner,
             device_id_type=MESH,
-        )
-
-    def send_term(k):
-        with jax.named_scope("term_send"):
-            term_send[k] = term(at(y, ahead(k)), 1 - core).astype(BF16)
-        term_copy(k).start()
-
-    def ahead(k):
-        return jnp.where(k == 0, 2, jnp.where(k == 1, 1, jnp.where(k == 2, 3, 0)))
+        ).start()
+
+    def own_term(k, rows, sem):
+        with jax.named_scope("term_own"):
+            y_index = at(y, AHEAD[k])
+            made = term(y_index, core, rows)
+            await_bytes(term_recv.at[k, rows], term_rs.at[sem])
+            term_own[y_index, rows] = (made + term_recv[k, rows].astype(F32)).astype(BF16)
 
     def bias_send(buffer, me, targets, which):
         view = buffer.at[me]
@@ -342,7 +395,7 @@
             ).start()
 
     def bias_sums():
-        bias_x[x] = jnp.zeros((8, ROUND), F32)
+        bias_x[x] = jnp.zeros((8, TILE), F32)
         for h in range(HEADS):
             wide = jnp.concatenate([dsum[h], jnp.zeros((SPAN, ROUND - TILE), F32)], axis=1)
             rows = SPAN
@@ -356,11 +409,13 @@
             first = lax.broadcasted_iota(jnp.int32, (1, ROUND), 1)
             clipped = jnp.sum(jnp.where(first < TILE, sums, 0.0), axis=1, keepdims=True)
             placed = pltpu.roll(sums, TABLE - 1, 1)
-            bias_x[x, h : h + 1, :] = jnp.where(first == TABLE - 1, clipped, placed)
+            sums = jnp.where(first == TABLE - 1, clipped, placed)
+            for piece in range(3):
+                bias_x[x, 3 * h + piece : 3 * h + piece + 1, :] = sums[:, piece * TILE : (piece + 1) * TILE]
 
     def finish():
         with jax.named_scope("back_wait"):
-            back_copy.wait_recv()
+            await_bytes(back_recv, halo_recv.at[1])
             dkv[LENGTH:, :] = dkv[LENGTH:, :] + back_recv[...].astype(F32)
 
         def finish_chunk(chunk, carry):
@@ -374,50 +429,38 @@
         with jax.named_scope("finish"):
             lax.fori_loop(0, CHUNKS, finish_chunk, 0)
 
-    def weight_part(k):
+    def weight_row(k, z_index):
+        features = pl.ds(pl.multiple_of(z_index * RING * COLS, RING * COLS), RING * COLS)
+        made = dot(grads_t[k * COLS : (k + 1) * COLS, :], whole[:, features]).astype(BF16)
+        for x_index in range(RING):
+            cut = slice(x_index * COLS, (x_index + 1) * COLS)
+            part_b[k, z_index, x_index] = made[HEAD:, cut]
+
+            @pl.when(x_index != at(x, 2))
+            def _():
+                part_a[k, x_index, z_index] = made[:HEAD, cut]
+
+    def weight_far(k):
+        far_x = at(x, 2)
+        with jax.named_scope("weight_far"):
+            for z_index in range(RING):
+                features = pl.ds(pl.multiple_of(z_index * RING * COLS + far_x * COLS, COLS), COLS)
+                left = grads_t[k * COLS : k * COLS + HEAD, :]
+                part_a[k, far_x, z_index] = dot(left, whole[:, features]).astype(BF16)
+            first_ring(k, 0).start_far()
+            weight_row(k, at(z, 2))
+            first_ring(k, 1).start_far()
+
+    def weight_rest(k):
         def rows(i, inner):
-            z_index = at(z, 2 + i)
-            left = grads_t[pl.ds(pl.multiple_of(k * COLS, COLS), COLS), :]
-            features = pl.ds(pl.multiple_of(z_index * RING * COLS, RING * COLS), RING * COLS)
-            made = dot(left, whole[:, features]).astype(BF16)
-            for x_index in range(RING):
-                cut = slice(x_index * COLS, (x_index + 1) * COLS)
-                part_b[k, z_index, x_index] = made[HEAD:, cut]
-
-                @pl.when((k > 0) | (x_index != at(x, 2)))
-                def _():
-                    part_a[k, x_index, z_index] = made[:HEAD, cut]
-
-            @pl.when(i == 0)
-            def _():
-                first_ring(k, 1).start_far()
-
+            weight_row(k, at(z, i))
             return inner
 
-        with jax.named_scope("weight_rows"):
-            lax.fori_loop(0, RING, rows, 0)
-
-        @pl.when(k > 0)
-        def _():
-            first_ring(k, 0).start_far()
-
+        with jax.named_scope("weight_rest"):
+            lax.fori_loop(3, RING + 2, rows, 0)
         for side in range(2):
             for d in range(2):
                 first_ring(k, side).start_near(d)
-
-    def own_term(k):
-        with jax.named_scope("term_own"):
-            y_index = at(y, ahead(k))
-            made = term(y_index, core)
-            term_copy(k).wait_recv()
-            term_own[y_index] = (made + term_recv[k].astype(F32)).astype(BF16)
-
-    with jax.named_scope("weight_first"):
-        far_x = at(x, 2)
-        for z_index in range(RING):
-            features = pl.ds(pl.multiple_of(z_index * RING * COLS + far_x * COLS, COLS), COLS)
-            part_a[0, far_x, z_index] = dot(grads_t[0:HEAD, :], whole[:, features]).astype(BF16)
-        first_ring(0, 0).start_far()
 
     def first_join(p):
         with jax.named_scope("join_first"):
@@ -425,53 +468,39 @@
             for side in range(2):
                 first_ring(p, side).join()
 
-    def reduce_step(k, carry):
-        @pl.when(k < 3)
-        def _():
-            weight_part(k)
-
-        @pl.when(k == 0)
-        def _():
-            finish()
-            with jax.named_scope("bias_sums"):
-                bias_sums()
-            bias_send(bias_x, x, [at_x(by) for by in (1, 2, 3)], 0)
-
-        @pl.when(k >= 1)
-        def _():
-            own_term(k - 1)
-
-        @pl.when(k == 1)
-        def _():
-            y_ring.start_far()
-
-        for d in range(2):
-            @pl.when(k == 2 + d)
-            def _():
-                y_ring.start_near(d)
-
-        @pl.when(k < RING)
-        def _():
-            send_term(k)
-
-        @pl.when((k >= 1) & (k < 3))
-        def _():
-            first_join(k - 1)
-
-        @pl.when(k == 3)
-        def _():
-            with jax.named_scope("bias_x"):
-                await_bytes(bias_x.at[0:3], bias_rs.at[0])
-                bias_z[z] = (bias_x[0] + bias_x[1]) + (bias_x[2] + bias_x[3])
-                bias_send(bias_z, z, [at_z(by) for by in (1, 2, 3)], 1)
-
-        return carry
-
-    lax.fori_loop(0, RING + 1, reduce_step, 0)
-
+    whole_rows = slice(0, LENGTH)
+    weight_far(0)
+    weight_rest(0)
+    finish()
+    for half in range(2):
+        send_term(0, halves[half], half)
+    weight_far(1)
+    for half in range(2):
+        own_term(0, halves[half], half)
+        y_ring.start(0, half)
+    send_term(1, whole_rows, 2)
+    weight_rest(1)
+    first_join(0)
+    with jax.named_scope("bias_sums"):
+        bias_sums()
+    bias_send(bias_x, x, [at_x(by) for by in (1, 2, 3)], 0)
+    own_term(1, whole_rows, 2)
+    y_ring.start_near(0)
+    weight_far(2)
+    send_term(2, whole_rows, 3)
+    send_term(3, whole_rows, 4)
+    own_term(2, whole_rows, 3)
+    y_ring.start_near(1)
+    weight_rest(2)
+    first_join(1)
     with jax.named_scope("join_y"):
         await_bytes(far_y, y_rs.at[0])
         y_ring.join()
+    with jax.named_scope("bias_x"):
+        await_bytes(bias_x.at[0:3], bias_rs.at[0])
+        bias_z[z] = (bias_x[0] + bias_x[1]) + (bias_x[2] + bias_x[3])
+    bias_send(bias_z, z, [at_z(by) for by in (1, 2, 3)], 1)
+    own_term(3, whole_rows, 4)
 
     def second_start(p):
         with jax.named_scope(f"second_start_{p}"):
@@ -510,7 +539,11 @@
     second_finish(0)
     with jax.named_scope("bias_z"):
         await_bytes(bias_z.at[0:3], bias_rs.at[1])
-        bias_out[...] = ((bias_z[0] + bias_z[1]) + (bias_z[2] + bias_z[3]))[:HEADS, :TABLE]
+        sums = (bias_z[0] + bias_z[1]) + (bias_z[2] + bias_z[3])
+        for h in range(HEADS):
+            for piece in range(3):
+                cut = slice(piece * TILE, min((piece + 1) * TILE, TABLE))
+                bias_out[h : h + 1, cut] = sums[3 * h + piece : 3 * h + piece + 1, : cut.stop - cut.start]
     second_join(2)
     second_finish(1)
     with jax.named_scope("input_sum"):
@@ -536,24 +569,35 @@
         await_bytes(bias_z.at[0:3], sent.at[9])
 
 
+def store_results(*refs):
+    sources, targets, sems = refs[:5], refs[5:10], refs[10]
+    copies = [pltpu.make_async_copy(source, target, sems.at[n]) for n, (source, target) in enumerate(zip(sources, targets))]
+    for copy in copies:
+        copy.start()
+    for copy in copies:
+        copy.wait()
+
+
 def shards(tokens, query_weight, key_weight, value_weight, position_bias, out_grad):
     anywhere = pl.BlockSpec(memory_space=pl.ANY)
     near = pl.BlockSpec(memory_space=pltpu.VMEM)
     dma = pltpu.SemaphoreType.DMA
     vmem = pltpu.VMEM
     grad = vmem((COLS, COLS), F32)
-    return pl.pallas_call(
+    results = pl.pallas_call(
         kernel,
         name="segment_attention_grads",
         out_shape=(
             vmem((LENGTH, FEATURES), BF16), grad, grad, grad,
             vmem((HEADS, TABLE), F32),
         ),
-        in_specs=[anywhere, anywhere, anywhere, anywhere, near, anywhere],
+        in_specs=[anywhere] * 6,
         out_specs=(near,) * 5,
         scratch_shapes=[
+            vmem((HEADS, TABLE), F32),
             vmem((LENGTH, WIDTH), BF16),
             vmem((WIDTH, 3 * COLS), BF16),
+            vmem((TILE, 3 * COLS), F32),
             vmem((LENGTH, COLS), BF16),
             vmem((REACH + LENGTH, 2 * COLS), BF16),
             vmem((LENGTH, COLS), BF16),
@@ -576,12 +620,12 @@
             vmem((2, 2, LENGTH // 2, FEATURES), BF16),
             vmem((HEADS, SPAN, TILE), F32),
             vmem((HEADS, SPAN, TILE), F32),
-            vmem((RING, 8, ROUND), F32),
-            vmem((RING, 8, ROUND), F32),
-            dma((5,)),
-            dma((CHUNKS,)), dma((CHUNKS,)), dma((CHUNKS,)),
+            vmem((RING, 8, TILE), F32),
+            vmem((RING, 8, TILE), F32),
+            dma((8,)),
+            dma((CHUNKS,)), dma((CHUNKS,)), dma((CHUNKS,)), dma((CHUNKS,)), dma((CHUNKS,)),
             dma((3,)),
-            dma((RING,)),
+            dma((RING + 1,)),
             dma((3, 2)), dma((3, 2)), dma((2,)),
             dma((2,)),
             dma((10,)),
@@ -590,6 +634,15 @@
             collective_id=0, has_side_effects=True, vmem_limit_bytes=62_000_000
         ),
     )(tokens, query_weight, key_weight, value_weight, position_bias, out_grad)
+    return pl.pallas_call(
+        store_results,
+        name="store_results",
+        out_shape=tuple(jax.ShapeDtypeStruct(result.shape, result.dtype) for result in results),
+        in_specs=[near] * 5,
+        out_specs=(anywhere,) * 5,
+        scratch_shapes=[dma((5,))],
+        compiler_params=pltpu.CompilerParams(vmem_limit_bytes=1_000_000),
+    )(*results)
 
 
 def solution(mesh):

time: 85.4 us -> 80.7 us (0.945)
  local copies, waits for them, and re-layouts: 3.57 us -> 0 us
  Pallas kernels: 81 us -> 78.9 us
    unnamed x5 -> x0, local copies, waits for them, and re-layouts: 3.57 us -> none
    pallas_call x1, Pallas kernels: 81 us -> 77.7 us  [shards(): pl.pallas_call(kernel, name='segment_attention_grads', out_shape=(vmem((L...]
    pallas_call x0 -> x1, Pallas kernels: none -> 1.18 us  [shards(): pl.pallas_call(store_results, name='store_results', out_shape=tuple((jax....]
where the time goes in v2:
time: 80.7 us; the launch traced here: 79.7 us
  Pallas kernels  78.9 us (98%)
    pallas_call x1, Pallas kernels, shards(): pl.pallas_call(kernel, name='segment_attention_grads', out_shape=(vmem((L...  77.7 us

profile of v2, /device:TPU:1, one launch (start us, length us, event | category | flops | bytes accessed | tf_op | source)
XLA Modules:
  0.0 79.7 jit_solution(15714161666995757553)
XLA Ops:
  0.6 77.7 %segment_attention_grads.1 = (bf16[768,512]{1,0:T(8,128)(2,1)S(1)}, f32[256,256]{1,0:T(8,128)S(1)}, f32[256,256]{1,0:T(8,128)S(1)}, f32[256,256]{1,0:T(8,128)S(1)}, f32[2,320]{1,0:T(2,128)S(1)}) custom-call(bf16[768,512]{1,0:T(8,128)(2,1)} %tokens.1, bf16[4096,256]{1,0:T(8,128)(2,1)} %wq.1, bf16[4096,256]{1,0:T(8,128)(2,1)} %wk.1, bf16[4096,256]{1,0:T(8,128)(2,1)} %wv.1, ...), custom_call_target="tpu_custom_call" | custom-call | tf_op jit(solution)/shard_map/segment_attention_grads/pallas_call | solution.py:587
  78.3 1.2 %store_results.1 = (bf16[768,512]{1,0:T(8,128)(2,1)}, f32[256,256]{1,0:T(8,128)}, f32[256,256]{1,0:T(8,128)}, f32[256,256]{1,0:T(8,128)}, f32[2,320]{1,0:T(2,128)}) custom-call(bf16[768,512]{1,0:T(8,128)(2,1)S(1)} %get-tuple-element.10.refs_0_, f32[256,256]{1,0:T(8,128)S(1)} %get-tuple-element.11.refs_1_, f32[256,256]{1,0:T(8,128)S(1)} %get-tuple-element.12.refs_2_, ...), custom_call_target="tpu_custom_call" | custom-call | tf_op jit(solution)/shard_map/store_results/pallas_call | solution.py:637

commit v3 on v2

--- a/solution.py
+++ b/solution.py
@@ -21,6 +21,7 @@
 TABLE = 320
 ROUND = 512
 AHEAD = (2, 1, 3, 0)
+STRAIGHT = (2,)
 
 
 def dot(left, right, left_dim=1, right_dim=0):
@@ -46,6 +47,20 @@
             device_id_type=MESH,
         ).start()
 
+    def start_straight(self, opposite):
+        for d in range(2):
+            pltpu.make_async_remote_copy(
+                src_ref=self.block(self.far, d),
+                dst_ref=self.landing[0](d),
+                send_sem=self.sent,
+                recv_sem=self.arrived[0],
+                device_id=opposite,
+                device_id_type=MESH,
+            ).start()
+        for kind in (1, 2):
+            for d in range(2):
+                self.start(kind, d)
+
     def start_far(self):
         for d in range(2):
             self.start(0, d)
@@ -71,7 +86,7 @@
 def kernel(
     tokens, wq, wk, wv, position_bias, out_grad,
     input_out, wq_out, wk_out, wv_out, bias_out,
-    table, whole, weight, projected, query, kv, upstream, dkv, grads, grads_t, back_send, back_recv,
+    table, whole, weight, projected, query, kv, upstream, keys_t, dkv, grads, grads_t, back_send, back_recv,
     part_a, part_b, far_ab, near_join, second_ab, far2_ab, near_join2,
     term_own, term_send, term_recv, far_y, near_join_y,
     bias, dsum, bias_x, bias_z,
@@ -198,11 +213,9 @@
         for h in range(HEADS):
             cols, value_cols, keys, asked, given = heads[h][:5]
             weights_low, score_low = lows[h]
+            grads_t[cols, here] = (dot(keys_t[cols, keys_at], score_low) * FACTOR).astype(BF16)
             dkv[keys_at, value_cols] = dkv[keys_at, value_cols] + dot(weights_low, given)
             dkv[keys_at, cols] = dkv[keys_at, cols] + dot(score_low, asked)
-            query_grad = dot(score_low, keys, 0, 0) * FACTOR
-            grads[here, cols] = query_grad.astype(BF16)
-            grads_t[cols, here] = query_grad.T.astype(BF16)
 
     for step in range(2):
         own_loads[step].wait()
@@ -252,6 +265,12 @@
             await_bytes(whole.at[0:TILE, 0:FEATURES], hop_recv.at[step])
             core_copy(step, 3).start()
 
+    def project_most(step):
+        with jax.named_scope("core_wait"):
+            await_bytes(whole.at[0:TILE, 0 : 3 * FEATURES], core_recv.at[step])
+        with jax.named_scope("project"):
+            projected[lax.rem(step, 2)] = project_from(step, (0, 1, 2))
+
     def gather_step(s, carry):
         @pl.when(s < CHUNKS)
         def _():
@@ -265,16 +284,9 @@
             gather_start(s + 2)
             core_copy(s + 2, 0).start()
 
-        @pl.when(s == CHUNKS)
-        def _():
-            hop_landed(s - 1)
-
-        @pl.when(s >= 1)
-        def _():
-            with jax.named_scope("core_wait"):
-                await_bytes(whole.at[0:TILE, 0 : 3 * FEATURES], core_recv.at[s - 1])
-            with jax.named_scope("project"):
-                projected[...] = project_from(s - 1, (0, 1, 2))
+        @pl.when((s >= 1) & (s < CHUNKS))
+        def _():
+            project_most(s - 1)
 
         @pl.when(s < CHUNKS)
         def _():
@@ -283,14 +295,19 @@
                 for d in range(2):
                     core_copy(s, 1 + d).start()
 
-        @pl.when((s >= 1) & (s < CHUNKS))
+        @pl.when(s >= 1)
         def _():
             hop_landed(s - 1)
+
+        @pl.when(s == CHUNKS - 1)
+        def _():
+            project_most(s)
 
         @pl.when(s == 4)
         def _():
             with jax.named_scope("halo_wait"):
                 await_bytes(kv.at[0:REACH, :], halo_recv.at[0])
+                keys_t[:, 0:REACH] = kv[0:REACH, :COLS].T
 
         @pl.when((s == 4) | (s == 6))
         def _():
@@ -307,9 +324,10 @@
                 await_bytes(whole.at[0:TILE, 0:FEATURES], last_recv.at[s - 1])
             with jax.named_scope("project_rest"):
                 start = rows_of(s - 1)
-                low = (projected[...] + project_from(s - 1, (3,))).astype(BF16)
+                low = (projected[lax.rem(s - 1, 2)] + project_from(s - 1, (3,))).astype(BF16)
                 query[pl.ds(start, TILE), :] = low[:, :COLS]
                 kv[pl.ds(pl.multiple_of(start + REACH, TILE), TILE), :] = low[:, COLS:]
+                keys_t[:, pl.ds(pl.multiple_of(start + REACH, TILE), TILE)] = low[:, COLS : 2 * COLS].T
 
         @pl.when((s >= 1) & (s <= 2))
         def _():
@@ -420,6 +438,7 @@
 
         def finish_chunk(chunk, carry):
             start = pl.multiple_of(chunk * TILE, TILE)
+            grads[pl.ds(start, TILE), :COLS] = grads_t[:COLS, pl.ds(start, TILE)].T
             total = dkv[pl.ds(pl.multiple_of(start + REACH, TILE), TILE), :]
             total = jnp.concatenate([total[:, :COLS] * FACTOR, total[:, COLS:]], axis=1)
             grads[pl.ds(start, TILE), COLS:] = total.astype(BF16)
@@ -478,17 +497,17 @@
     for half in range(2):
         own_term(0, halves[half], half)
         y_ring.start(0, half)
-    send_term(1, whole_rows, 2)
     weight_rest(1)
     first_join(0)
+    send_term(1, whole_rows, 2)
     with jax.named_scope("bias_sums"):
         bias_sums()
     bias_send(bias_x, x, [at_x(by) for by in (1, 2, 3)], 0)
-    own_term(1, whole_rows, 2)
-    y_ring.start_near(0)
     weight_far(2)
     send_term(2, whole_rows, 3)
     send_term(3, whole_rows, 4)
+    own_term(1, whole_rows, 2)
+    y_ring.start_near(0)
     own_term(2, whole_rows, 3)
     y_ring.start_near(1)
     weight_rest(2)
@@ -510,6 +529,10 @@
                 for half in range(2):
                     second_ab[p, side, 2 * half : 2 * half + 2] = ring.half(half).astype(BF16)
             rings = [second_ring(p, side) for side in range(2)]
+            if p in STRAIGHT:
+                rings[0].start_straight(at_z(2))
+                rings[1].start_straight(at_x(2))
+                return
             for ring in rings:
                 ring.start_far()
             for ring in rings:
@@ -525,13 +548,18 @@
     def second_finish(p):
         with jax.named_scope(f"second_finish_{p}"):
             await_bytes(near_join2.at[p], second_rs.at[p, 1])
+            if p in STRAIGHT:
+                await_bytes(far2_ab.at[p], second_rs.at[p, 0])
             for side in range(2):
                 ring = second_ring(p, side)
-                total = jnp.concatenate([ring.half(0), ring.half(1)], axis=0)
+                sums = [ring.half(half) for half in range(2)]
+                if p in STRAIGHT:
+                    sums = [sums[half] + far2_ab[p, side, half].astype(F32) for half in range(2)]
+                total = jnp.concatenate(sums, axis=0)
                 (wq_out, wk_out, wv_out)[p][:, side * HEAD : (side + 1) * HEAD] = total.T
 
+    first_join(2)
     second_start(0)
-    first_join(2)
     second_start(1)
     second_join(0)
     second_start(2)
@@ -544,12 +572,11 @@
             for piece in range(3):
                 cut = slice(piece * TILE, min((piece + 1) * TILE, TABLE))
                 bias_out[h : h + 1, cut] = sums[3 * h + piece : 3 * h + piece + 1, : cut.stop - cut.start]
-    second_join(2)
-    second_finish(1)
     with jax.named_scope("input_sum"):
         await_bytes(near_join_y, y_rs.at[1])
         for d in range(2):
             input_out[d * (LENGTH // 2) : (d + 1) * (LENGTH // 2), :] = y_ring.half(d).astype(BF16)
+    second_finish(1)
     second_finish(2)
 
     with jax.named_scope("drain"):
@@ -597,10 +624,11 @@
             vmem((HEADS, TABLE), F32),
             vmem((LENGTH, WIDTH), BF16),
             vmem((WIDTH, 3 * COLS), BF16),
-            vmem((TILE, 3 * COLS), F32),
+            vmem((2, TILE, 3 * COLS), F32),
             vmem((LENGTH, COLS), BF16),
             vmem((REACH + LENGTH, 2 * COLS), BF16),
             vmem((LENGTH, COLS), BF16),
+            vmem((COLS, REACH + LENGTH), BF16),
             vmem((REACH + LENGTH, 2 * COLS), F32),
             vmem((LENGTH, 3 * COLS), BF16),
             vmem((3 * COLS, LENGTH), BF16),

time: 80.7 us -> 79.2 us (0.981); the launches traced: 79.7 us -> 79.1 us
  no operation moved by 1% of the time
where the time goes in v3:
time: 79.2 us; the launch traced here: 79.1 us
  Pallas kernels  78.3 us (99%)
  between operations  0.8 us (1%)
    pallas_call x1, Pallas kernels, shards(): pl.pallas_call(kernel, name='segment_attention_grads', out_shape=(vmem((L...  77.1 us

profile of v3, /device:TPU:1, one launch (start us, length us, event | category | flops | bytes accessed | tf_op | source)
XLA Modules:
  0.0 79.1 jit_solution(9791695494897671770)
XLA Ops:
  0.6 77.1 %segment_attention_grads.1 = (bf16[768,512]{1,0:T(8,128)(2,1)S(1)}, f32[256,256]{1,0:T(8,128)S(1)}, f32[256,256]{1,0:T(8,128)S(1)}, f32[256,256]{1,0:T(8,128)S(1)}, f32[2,320]{1,0:T(2,128)S(1)}) custom-call(bf16[768,512]{1,0:T(8,128)(2,1)} %tokens.1, bf16[4096,256]{1,0:T(8,128)(2,1)} %wq.1, bf16[4096,256]{1,0:T(8,128)(2,1)} %wk.1, bf16[4096,256]{1,0:T(8,128)(2,1)} %wv.1, ...), custom_call_target="tpu_custom_call" | custom-call | tf_op jit(solution)/shard_map/segment_attention_grads/pallas_call | solution.py:614
  77.8 1.2 %store_results.1 = (bf16[768,512]{1,0:T(8,128)(2,1)}, f32[256,256]{1,0:T(8,128)}, f32[256,256]{1,0:T(8,128)}, f32[256,256]{1,0:T(8,128)}, f32[2,320]{1,0:T(2,128)}) custom-call(bf16[768,512]{1,0:T(8,128)(2,1)S(1)} %get-tuple-element.10.refs_0_, f32[256,256]{1,0:T(8,128)S(1)} %get-tuple-element.11.refs_1_, f32[256,256]{1,0:T(8,128)S(1)} %get-tuple-element.12.refs_2_, ...), custom_call_target="tpu_custom_call" | custom-call | tf_op jit(solution)/shard_map/store_results/pallas_call | solution.py:665

commit v4 on v3

--- a/solution.py
+++ b/solution.py
@@ -18,6 +18,7 @@
 COLS = HEADS * HEAD
 FACTOR = HEAD ** (-0.5)
 RING = 4
+LOG2_E = 1.4426950408889634
 TABLE = 320
 ROUND = 512
 AHEAD = (2, 1, 3, 0)
@@ -187,35 +188,52 @@
     edge = jnp.where(sp == 0, REACH, 0)
     row = lax.broadcasted_iota(jnp.int32, (SPAN, TILE), 0)
 
-    def attend(tile):
+    def ranges(tile):
         start = tile * TILE if isinstance(tile, int) else pl.multiple_of(tile * TILE, TILE)
-        keys_at, here = pl.ds(start, SPAN), pl.ds(start, TILE)
-        heads = []
-        for h in range(HEADS):
-            cols = slice(h * HEAD, (h + 1) * HEAD)
-            value_cols = slice(COLS + h * HEAD, COLS + (h + 1) * HEAD)
-            keys, values = kv[keys_at, cols], kv[keys_at, value_cols]
-            asked, given = query[here, cols], upstream[here, cols]
-            heads.append((cols, value_cols, keys, asked, given, dot(keys, asked, 1, 1), dot(values, given, 1, 1)))
+        return start, pl.ds(start, SPAN), pl.ds(start, TILE)
+
+    head_cols = [slice(h * HEAD, (h + 1) * HEAD) for h in range(HEADS)]
+    value_cols = [slice(COLS + h * HEAD, COLS + (h + 1) * HEAD) for h in range(HEADS)]
+
+    def attend_products(tile):
+        _, keys_at, here = ranges(tile)
+        return [
+            (dot(kv[keys_at, head_cols[h]], query[here, head_cols[h]], 1, 1), dot(kv[keys_at, value_cols[h]], upstream[here, head_cols[h]], 1, 1))
+            for h in range(HEADS)
+        ]
+
+    def attend_weights(tile, products):
+        start, _, _ = ranges(tile)
         lows = []
         for h in range(HEADS):
-            scores = heads[h][5] * FACTOR + bias[h]
+            raw, prob_grad = products[h]
+            scores = raw * (FACTOR * LOG2_E) + bias[h]
             if not isinstance(tile, int):
                 scores = jnp.where(row + start < edge, -jnp.inf, scores)
-            top = jnp.max(scores, axis=0, keepdims=True)
-            raised = jnp.exp(scores - top)
+            raised = jnp.exp2(scores - jnp.max(scores, axis=0, keepdims=True))
             weights = raised * (1.0 / jnp.sum(raised, axis=0, keepdims=True))
-            prob_grad = heads[h][6]
             delta = jnp.sum(weights * prob_grad, axis=0, keepdims=True)
             score_grad = weights * (prob_grad - delta)
             dsum[h] = dsum[h] + score_grad
             lows.append((weights.astype(BF16), score_grad.astype(BF16)))
+        return lows
+
+    def attend_queries(tile, lows):
+        _, keys_at, here = ranges(tile)
         for h in range(HEADS):
-            cols, value_cols, keys, asked, given = heads[h][:5]
+            grads_t[head_cols[h], here] = (dot(keys_t[head_cols[h], keys_at], lows[h][1]) * FACTOR).astype(BF16)
+
+    def attend_keys(tile, lows):
+        _, keys_at, here = ranges(tile)
+        for h in range(HEADS):
             weights_low, score_low = lows[h]
-            grads_t[cols, here] = (dot(keys_t[cols, keys_at], score_low) * FACTOR).astype(BF16)
-            dkv[keys_at, value_cols] = dkv[keys_at, value_cols] + dot(weights_low, given)
-            dkv[keys_at, cols] = dkv[keys_at, cols] + dot(score_low, asked)
+            dkv[keys_at, value_cols[h]] = dkv[keys_at, value_cols[h]] + dot(weights_low, upstream[here, head_cols[h]])
+            dkv[keys_at, head_cols[h]] = dkv[keys_at, head_cols[h]] + dot(score_low, query[here, head_cols[h]])
+
+    def attend(tile):
+        lows = attend_weights(tile, attend_products(tile))
+        attend_queries(tile, lows)
+        attend_keys(tile, lows)
 
     for step in range(2):
         own_loads[step].wait()
@@ -244,7 +262,7 @@
         last = jnp.broadcast_to(table[h : h + 1, TABLE - 1 : TABLE], (8, ROUND))
         turned = jnp.where(lane < TILE, last, turned)
         skewed = pltpu.roll(jnp.broadcast_to(turned[0:1, :], (SPAN, ROUND)), 0, 1, stride=1, stride_axis=0)
-        bias[h] = jnp.where(seen, skewed[:, :TILE], -jnp.inf)
+        bias[h] = jnp.where(seen, skewed[:, :TILE] * LOG2_E, -jnp.inf)
         dsum[h] = jnp.zeros((SPAN, TILE), F32)
     dkv[...] = jnp.zeros(dkv.shape, F32)
 
@@ -343,8 +361,15 @@
 
     lax.fori_loop(0, CHUNKS + 1, gather_step, 0)
     with jax.named_scope("attend_last"):
-        for tile in range(3, CHUNKS):
-            attend(tile)
+        products = {tile: attend_products(tile) for tile in (3, 4)}
+        lows = {3: attend_weights(3, products[3])}
+        products[5] = attend_products(5)
+        attend_queries(3, lows[3])
+        for tile in (4, 5):
+            lows[tile] = attend_weights(tile, products[tile])
+            attend_queries(tile, lows[tile])
+            attend_keys(tile - 1, lows[tile - 1])
+        attend_keys(5, lows[5])
 
     def first_ring(p, side):
         me = (x, z)[side]

time: 79.2 us -> 78.9 us (level)
  no operation moved by 1% of the time
where the time goes in v4:
time: 78.9 us; the launch traced here: 78.8 us
  Pallas kernels  78 us (99%)
  between operations  0.8 us (1%)
    pallas_call x1, Pallas kernels, shards(): pl.pallas_call(kernel, name='segment_attention_grads', out_shape=(vmem((L...  76.8 us

profile of v4, /device:TPU:1, one launch (start us, length us, event | category | flops | bytes accessed | tf_op | source)
XLA Modules:
  0.0 78.8 jit_solution(1318996164353342200)
XLA Ops:
  0.6 76.8 %segment_attention_grads.1 = (bf16[768,512]{1,0:T(8,128)(2,1)S(1)}, f32[256,256]{1,0:T(8,128)S(1)}, f32[256,256]{1,0:T(8,128)S(1)}, f32[256,256]{1,0:T(8,128)S(1)}, f32[2,320]{1,0:T(2,128)S(1)}) custom-call(bf16[768,512]{1,0:T(8,128)(2,1)} %tokens.1, bf16[4096,256]{1,0:T(8,128)(2,1)} %wq.1, bf16[4096,256]{1,0:T(8,128)(2,1)} %wk.1, bf16[4096,256]{1,0:T(8,128)(2,1)} %wv.1, ...), custom_call_target="tpu_custom_call" | custom-call | tf_op jit(solution)/shard_map/segment_attention_grads/pallas_call | solution.py:639
  77.4 1.2 %store_results.1 = (bf16[768,512]{1,0:T(8,128)(2,1)}, f32[256,256]{1,0:T(8,128)}, f32[256,256]{1,0:T(8,128)}, f32[256,256]{1,0:T(8,128)}, f32[2,320]{1,0:T(2,128)}) custom-call(bf16[768,512]{1,0:T(8,128)(2,1)S(1)} %get-tuple-element.10.refs_0_, f32[256,256]{1,0:T(8,128)S(1)} %get-tuple-element.11.refs_1_, f32[256,256]{1,0:T(8,128)S(1)} %get-tuple-element.12.refs_2_, ...), custom_call_target="tpu_custom_call" | custom-call | tf_op jit(solution)/shard_map/store_results/pallas_call | solution.py:690

commit v5 on v4

--- a/solution.py
+++ b/solution.py
@@ -156,18 +156,18 @@
     def hop_copy(step, d):
         cols = feature_cols(at(y, (3, 1)[d]), core)
         rows = pl.ds(pl.multiple_of(rows_of(step) + d * SEGMENT, SEGMENT), SEGMENT)
-        return chunk_copy(rows, cols, (up, down)[d], sent.at[1], hop_recv.at[step])
+        return chunk_copy(rows, cols, (up, down)[d], sent.at[0], hop_recv.at[step])
 
     def core_copy(step, which):
         cols = feature_cols(at(y, (0, 3, 1, 2)[which]), core)
         sem = (last_recv if which == 3 else core_recv).at[step]
-        return chunk_copy(pl.ds(rows_of(step), TILE), cols, partner, sent.at[2], sem)
+        return chunk_copy(pl.ds(rows_of(step), TILE), cols, partner, sent.at[0], sem)
 
     def halo_copy(step):
         return pltpu.make_async_remote_copy(
             src_ref=kv.at[pl.ds(pl.multiple_of(LENGTH + step * TILE, TILE), TILE), :],
             dst_ref=kv.at[pl.ds(pl.multiple_of(step * TILE, TILE), TILE), :],
-            send_sem=sent.at[3],
+            send_sem=sent.at[0],
             recv_sem=halo_recv.at[0],
             device_id=at_sp(1),
             device_id_type=MESH,
@@ -179,7 +179,7 @@
         pltpu.make_async_remote_copy(
             src_ref=back_send.at[rows],
             dst_ref=back_recv.at[rows],
-            send_sem=sent.at[4],
+            send_sem=sent.at[0],
             recv_sem=halo_recv.at[1],
             device_id=at_sp(15),
             device_id_type=MESH,
@@ -241,12 +241,12 @@
         core_copy(step, 0).start()
     own_loads[2].wait()
 
-    table_load = pltpu.make_async_copy(position_bias, table, load_sem.at[7])
+    table_load = pltpu.make_async_copy(position_bias, table, load_sem.at[5])
     table_load.start()
     loads = []
     for number, ref in enumerate((wq, wk, wv)):
-        loads.append(pltpu.make_async_copy(ref, weight.at[:, number * COLS : (number + 1) * COLS], load_sem.at[3 + number]))
-    loads.append(pltpu.make_async_copy(out_grad, upstream, load_sem.at[6]))
+        loads.append(pltpu.make_async_copy(ref, weight.at[:, number * COLS : (number + 1) * COLS], load_sem.at[3]))
+    loads.append(pltpu.make_async_copy(out_grad, upstream, load_sem.at[4]))
     for load in loads:
         load.start()
 
@@ -266,8 +266,8 @@
         dsum[h] = jnp.zeros((SPAN, TILE), F32)
     dkv[...] = jnp.zeros(dkv.shape, F32)
 
-    for load in loads:
-        load.wait()
+    await_bytes(weight, load_sem.at[3])
+    loads[3].wait()
 
     def project_from(step, blocks):
         total = None
@@ -381,7 +381,7 @@
             lambda d: far_ab.at[p, side, d],
             lambda d: near_join.at[p, 0, side, d],
             lambda d: near_join.at[p, 1, side, d],
-            sent.at[5], ring_rs.at[p, 0], ring_rs.at[p, 1],
+            sent.at[0], ring_rs.at[p, 0], ring_rs.at[p, 1],
         )
 
     def second_ring(p, side):
@@ -393,7 +393,7 @@
             lambda d: far2_ab.at[p, side, d],
             lambda d: near_join2.at[p, 0, side, d],
             lambda d: near_join2.at[p, 1, side, d],
-            sent.at[6], second_rs.at[p, 0], second_rs.at[p, 1],
+            sent.at[0], second_rs.at[p, 0], second_rs.at[p, 1],
         )
 
     y_ring = Ring(
@@ -402,7 +402,7 @@
         lambda d: far_y.at[d],
         lambda d: near_join_y.at[0, d],
         lambda d: near_join_y.at[1, d],
-        sent.at[7], y_rs.at[0], y_rs.at[1],
+        sent.at[0], y_rs.at[0], y_rs.at[1],
     )
 
     halves = (slice(0, LENGTH // 2), slice(LENGTH // 2, LENGTH))
@@ -417,7 +417,7 @@
         pltpu.make_async_remote_copy(
             src_ref=term_send.at[k, rows],
             dst_ref=term_recv.at[k, rows],
-            send_sem=sent.at[8],
+            send_sem=sent.at[0],
             recv_sem=term_rs.at[sem],
             device_id=partner,
             device_id_type=MESH,
@@ -434,7 +434,7 @@
         view = buffer.at[me]
         for target in targets:
             pltpu.make_async_remote_copy(
-                src_ref=view, dst_ref=view, send_sem=sent.at[9], recv_sem=bias_rs.at[which], device_id=target, device_id_type=MESH
+                src_ref=view, dst_ref=view, send_sem=sent.at[0], recv_sem=bias_rs.at[which], device_id=target, device_id_type=MESH
             ).start()
 
     def bias_sums():
@@ -479,10 +479,7 @@
         for x_index in range(RING):
             cut = slice(x_index * COLS, (x_index + 1) * COLS)
             part_b[k, z_index, x_index] = made[HEAD:, cut]
-
-            @pl.when(x_index != at(x, 2))
-            def _():
-                part_a[k, x_index, z_index] = made[:HEAD, cut]
+            part_a[k, jnp.where(x_index == at(x, 2), RING, x_index), z_index] = made[:HEAD, cut]
 
     def weight_far(k):
         far_x = at(x, 2)
@@ -606,19 +603,19 @@
 
     with jax.named_scope("drain"):
         await_bytes(whole.at[:, 0 : 2 * FEATURES], sent.at[0])
-        await_bytes(whole.at[:, 0:FEATURES], sent.at[1])
-        await_bytes(whole.at[:, 0 : 4 * FEATURES], sent.at[2])
-        await_bytes(kv.at[0:REACH, :], sent.at[3])
-        await_bytes(back_send, sent.at[4])
-        await_bytes(far_ab, sent.at[5])
-        await_bytes(near_join, sent.at[5])
-        await_bytes(far2_ab, sent.at[6])
-        await_bytes(near_join2, sent.at[6])
-        await_bytes(far_y, sent.at[7])
-        await_bytes(near_join_y, sent.at[7])
-        await_bytes(term_recv, sent.at[8])
-        await_bytes(bias_x.at[0:3], sent.at[9])
-        await_bytes(bias_z.at[0:3], sent.at[9])
+        await_bytes(whole.at[:, 0:FEATURES], sent.at[0])
+        await_bytes(whole.at[:, 0 : 4 * FEATURES], sent.at[0])
+        await_bytes(kv.at[0:REACH, :], sent.at[0])
+        await_bytes(back_send, sent.at[0])
+        await_bytes(far_ab, sent.at[0])
+        await_bytes(near_join, sent.at[0])
+        await_bytes(far2_ab, sent.at[0])
+        await_bytes(near_join2, sent.at[0])
+        await_bytes(far_y, sent.at[0])
+        await_bytes(near_join_y, sent.at[0])
+        await_bytes(term_recv, sent.at[0])
+        await_bytes(bias_x.at[0:3], sent.at[0])
+        await_bytes(bias_z.at[0:3], sent.at[0])
 
 
 def store_results(*refs):
@@ -659,7 +656,7 @@
             vmem((3 * COLS, LENGTH), BF16),
             vmem((REACH, 2 * COLS), BF16),
             vmem((REACH, 2 * COLS), BF16),
-            vmem((3, RING, RING, HEAD, COLS), BF16),
+            vmem((3, RING + 1, RING, HEAD, COLS), BF16),
             vmem((3, RING, RING, HEAD, COLS), BF16),
             vmem((3, 2, 2, 2, HEAD, COLS), BF16),
             vmem((3, 2, 2, 2, 2, HEAD, COLS), BF16),
@@ -675,13 +672,13 @@
             vmem((HEADS, SPAN, TILE), F32),
             vmem((RING, 8, TILE), F32),
             vmem((RING, 8, TILE), F32),
-            dma((8,)),
+            dma((6,)),
             dma((CHUNKS,)), dma((CHUNKS,)), dma((CHUNKS,)), dma((CHUNKS,)), dma((CHUNKS,)),
             dma((3,)),
             dma((RING + 1,)),
             dma((3, 2)), dma((3, 2)), dma((2,)),
             dma((2,)),
-            dma((10,)),
+            dma((1,)),
         ],
         compiler_params=pltpu.CompilerParams(
             collective_id=0, has_side_effects=True, vmem_limit_bytes=62_000_000

time: 78.9 us -> 78.7 us (level)
  no operation moved by 1% of the time
where the time goes in v5:
time: 78.7 us; the launch traced here: 78.6 us
  Pallas kernels  77.8 us (99%)
  between operations  0.8 us (1%)
    pallas_call x1, Pallas kernels, shards(): pl.pallas_call(kernel, name='segment_attention_grads', out_shape=(vmem((L...  76.6 us

profile of v5, /device:TPU:1, one launch (start us, length us, event | category | flops | bytes accessed | tf_op | source)
XLA Modules:
  0.0 78.6 jit_solution(4932716956323176140)
XLA Ops:
  0.6 76.6 %segment_attention_grads.1 = (bf16[768,512]{1,0:T(8,128)(2,1)S(1)}, f32[256,256]{1,0:T(8,128)S(1)}, f32[256,256]{1,0:T(8,128)S(1)}, f32[256,256]{1,0:T(8,128)S(1)}, f32[2,320]{1,0:T(2,128)S(1)}) custom-call(bf16[768,512]{1,0:T(8,128)(2,1)} %tokens.1, bf16[4096,256]{1,0:T(8,128)(2,1)} %wq.1, bf16[4096,256]{1,0:T(8,128)(2,1)} %wk.1, bf16[4096,256]{1,0:T(8,128)(2,1)} %wv.1, ...), custom_call_target="tpu_custom_call" | custom-call | tf_op jit(solution)/shard_map/segment_attention_grads/pallas_call | solution.py:636
  77.3 1.2 %store_results.1 = (bf16[768,512]{1,0:T(8,128)(2,1)}, f32[256,256]{1,0:T(8,128)}, f32[256,256]{1,0:T(8,128)}, f32[256,256]{1,0:T(8,128)}, f32[2,320]{1,0:T(2,128)}) custom-call(bf16[768,512]{1,0:T(8,128)(2,1)S(1)} %get-tuple-element.10.refs_0_, f32[256,256]{1,0:T(8,128)S(1)} %get-tuple-element.11.refs_1_, f32[256,256]{1,0:T(8,128)S(1)} %get-tuple-element.12.refs_2_, ...), custom_call_target="tpu_custom_call" | custom-call | tf_op jit(solution)/shard_map/store_results/pallas_call | solution.py:687

commit v6 on v5

--- a/solution.py
+++ b/solution.py
@@ -368,8 +368,6 @@
         for tile in (4, 5):
             lows[tile] = attend_weights(tile, products[tile])
             attend_queries(tile, lows[tile])
-            attend_keys(tile - 1, lows[tile - 1])
-        attend_keys(5, lows[5])
 
     def first_ring(p, side):
         me = (x, z)[side]
@@ -471,7 +469,7 @@
             return carry
 
         with jax.named_scope("finish"):
-            lax.fori_loop(0, CHUNKS, finish_chunk, 0)
+            lax.fori_loop(0, CHUNKS, finish_chunk, 0, unroll=True)
 
     def weight_row(k, z_index):
         features = pl.ds(pl.multiple_of(z_index * RING * COLS, RING * COLS), RING * COLS)
@@ -498,7 +496,7 @@
             return inner
 
         with jax.named_scope("weight_rest"):
-            lax.fori_loop(3, RING + 2, rows, 0)
+            lax.fori_loop(3, RING + 2, rows, 0, unroll=True)
         for side in range(2):
             for d in range(2):
                 first_ring(k, side).start_near(d)
@@ -511,6 +509,9 @@
 
     whole_rows = slice(0, LENGTH)
     weight_far(0)
+    with jax.named_scope("attend_keys"):
+        for tile in (3, 4, 5):
+            attend_keys(tile, lows[tile])
     weight_rest(0)
     finish()
     for half in range(2):

time: 78.7 us -> 78.5 us (level)
  no operation moved by 1% of the time
where the time goes in v6:
time: 78.5 us; the launch traced here: 78.4 us
  Pallas kernels  77.6 us (99%)
  between operations  0.8 us (1%)
    pallas_call x1, Pallas kernels, shards(): pl.pallas_call(kernel, name='segment_attention_grads', out_shape=(vmem((L...  76.4 us

profile of v6, /device:TPU:1, one launch (start us, length us, event | category | flops | bytes accessed | tf_op | source)
XLA Modules:
  0.0 78.4 jit_solution(17723286251581694377)
XLA Ops:
  0.6 76.4 %segment_attention_grads.1 = (bf16[768,512]{1,0:T(8,128)(2,1)S(1)}, f32[256,256]{1,0:T(8,128)S(1)}, f32[256,256]{1,0:T(8,128)S(1)}, f32[256,256]{1,0:T(8,128)S(1)}, f32[2,320]{1,0:T(2,128)S(1)}) custom-call(bf16[768,512]{1,0:T(8,128)(2,1)} %tokens.1, bf16[4096,256]{1,0:T(8,128)(2,1)} %wq.1, bf16[4096,256]{1,0:T(8,128)(2,1)} %wk.1, bf16[4096,256]{1,0:T(8,128)(2,1)} %wv.1, ...), custom_call_target="tpu_custom_call" | custom-call | tf_op jit(solution)/shard_map/segment_attention_grads/pallas_call | solution.py:637
  77.1 1.2 %store_results.1 = (bf16[768,512]{1,0:T(8,128)(2,1)}, f32[256,256]{1,0:T(8,128)}, f32[256,256]{1,0:T(8,128)}, f32[256,256]{1,0:T(8,128)}, f32[2,320]{1,0:T(2,128)}) custom-call(bf16[768,512]{1,0:T(8,128)(2,1)S(1)} %get-tuple-element.10.refs_0_, f32[256,256]{1,0:T(8,128)S(1)} %get-tuple-element.11.refs_1_, f32[256,256]{1,0:T(8,128)S(1)} %get-tuple-element.12.refs_2_, ...), custom_call_target="tpu_custom_call" | custom-call | tf_op jit(solution)/shard_map/store_results/pallas_call | solution.py:688

commit v7 on v6

--- a/solution.py
+++ b/solution.py
@@ -584,8 +584,8 @@
     first_join(2)
     second_start(0)
     second_start(1)
+    second_start(2)
     second_join(0)
-    second_start(2)
     second_join(1)
     second_finish(0)
     with jax.named_scope("bias_z"):

time: 78.5 us -> 78.4 us (level)
  no operation moved by 1% of the time
where the time goes in v7:
time: 78.4 us; the launch traced here: 78.3 us
  Pallas kernels  77.5 us (99%)
  between operations  0.8 us (1%)
    pallas_call x1, Pallas kernels, shards(): pl.pallas_call(kernel, name='segment_attention_grads', out_shape=(vmem((L...  76.3 us

profile of v7, /device:TPU:1, one launch (start us, length us, event | category | flops | bytes accessed | tf_op | source)
XLA Modules:
  0.0 78.3 jit_solution(11235288016871236000)
XLA Ops:
  0.6 76.3 %segment_attention_grads.1 = (bf16[768,512]{1,0:T(8,128)(2,1)S(1)}, f32[256,256]{1,0:T(8,128)S(1)}, f32[256,256]{1,0:T(8,128)S(1)}, f32[256,256]{1,0:T(8,128)S(1)}, f32[2,320]{1,0:T(2,128)S(1)}) custom-call(bf16[768,512]{1,0:T(8,128)(2,1)} %tokens.1, bf16[4096,256]{1,0:T(8,128)(2,1)} %wq.1, bf16[4096,256]{1,0:T(8,128)(2,1)} %wk.1, bf16[4096,256]{1,0:T(8,128)(2,1)} %wv.1, ...), custom_call_target="tpu_custom_call" | custom-call | tf_op jit(solution)/shard_map/segment_attention_grads/pallas_call | solution.py:637
  76.9 1.2 %store_results.1 = (bf16[768,512]{1,0:T(8,128)(2,1)}, f32[256,256]{1,0:T(8,128)}, f32[256,256]{1,0:T(8,128)}, f32[256,256]{1,0:T(8,128)}, f32[2,320]{1,0:T(2,128)}) custom-call(bf16[768,512]{1,0:T(8,128)(2,1)S(1)} %get-tuple-element.10.refs_0_, f32[256,256]{1,0:T(8,128)S(1)} %get-tuple-element.11.refs_1_, f32[256,256]{1,0:T(8,128)S(1)} %get-tuple-element.12.refs_2_, ...), custom_call_target="tpu_custom_call" | custom-call | tf_op jit(solution)/shard_map/store_results/pallas_call | solution.py:688
